TPU v7x, 128 devices: a whole 4x4x4 slice. The times are simulated.
128 devices in a mesh: rep: 16 (over z, x), fs: 4 (over y), tp: 2 (over core).
Axes of the slice: x: 4, y: 4, z: 4, core: 2. Of those that a mesh axis runs over, the one named last changes fastest.
Arguments:
- tokens_in: bfloat16 [32768, 2048], P(('rep', 'fs', 'tp')), may hold values from -6 to 6
- norm_gain: float32 [2048], replicated, may hold values from 0.1 to 1.9
- gate_weight: bfloat16 [2048, 3072], P(None, ('fs', 'tp')), may hold values from -0.125 to 0.125
- up_weight: bfloat16 [2048, 3072], P(None, ('fs', 'tp')), may hold values from -0.125 to 0.125
- down_weight: bfloat16 [3072, 2048], P(('fs', 'tp')), may hold values from -0.109375 to 0.109375
- out_grad: bfloat16 [32768, 2048], P(('rep', 'fs', 'tp')), may hold values from -24 to 24
Outputs:
- grad_in: bfloat16 [32768, 2048], P(('rep', 'fs', 'tp'))
- grad_gain: float32 [2048], replicated
- grad_gate: float32 [2048, 3072], P(None, ('fs', 'tp'))
- grad_up: float32 [2048, 3072], P(None, ('fs', 'tp'))
- grad_down: float32 [3072, 2048], P(('fs', 'tp'))
All inputs are finite; a program needn't handle non-finite values.
Results may differ from a plain program's by a relative error of at most 0.014.
Values may be sent and summed in bfloat16 or wider, within the bound.
A program may use at most 192 MiB of HBM per device.

v0:
```python
import jax
import jax.numpy as jnp
from jax import lax
from jax.sharding import PartitionSpec as P

norm_eps = 1e-06


def sent_to_all(value, axis):
    length = lax.axis_size(axis)
    return lax.all_to_all(
        jnp.broadcast_to(value[None], (length, *value.shape)), axis, 0, 0, tiled=True
    )


def taken_together(value, axis):
    return sent_to_all(value, axis).sum(axis=0)


def shards(tokens_in, norm_gain, gate_weight, up_weight, down_weight, out_grad):
    row_count = tokens_in.shape[0]
    total_tokens = row_count * lax.axis_size("rep") * lax.axis_size("fs") * lax.axis_size("tp")
    factor = float(total_tokens) ** (-0.5)
    whole_in, whole_grad = (
        lax.all_gather(tokens_in, ("fs", "tp"), axis=0, tiled=True),
        lax.all_gather(out_grad, ("fs", "tp"), axis=0, tiled=True),
    )
    floats = whole_in.astype(jnp.float32)
    inverse = lax.rsqrt(jnp.mean(floats * floats, axis=-1, keepdims=True) + norm_eps)
    unit_rows = floats * inverse
    normed = (unit_rows * norm_gain).astype(jnp.bfloat16)
    gate_pre = jnp.dot(normed, gate_weight, preferred_element_type=jnp.float32)
    up_pre = jnp.dot(normed, up_weight, preferred_element_type=jnp.float32)
    sigma = jax.nn.sigmoid(gate_pre)
    active = gate_pre * sigma
    hidden = (active * up_pre).astype(jnp.bfloat16)
    grad_hidden = 0.5 * jnp.dot(whole_grad, down_weight.T, preferred_element_type=jnp.float32)
    grad_gate_pre = (grad_hidden * up_pre * sigma * (1.0 + gate_pre * (1.0 - sigma))).astype(
        jnp.bfloat16
    )
    grad_up_pre = (grad_hidden * active).astype(jnp.bfloat16)
    result = jnp.dot(grad_gate_pre, gate_weight.T, preferred_element_type=jnp.float32)
    grad_normed = lax.psum_scatter(
        (result + jnp.dot(grad_up_pre, up_weight.T, preferred_element_type=jnp.float32)).astype(
            jnp.bfloat16
        ),
        ("fs", "tp"),
        scatter_dimension=0,
        tiled=True,
    ).astype(jnp.float32)
    local_gate = jnp.dot(normed.T, grad_gate_pre, preferred_element_type=jnp.float32)
    local_up = jnp.dot(normed.T, grad_up_pre, preferred_element_type=jnp.float32)
    local_down = jnp.dot(hidden.T, whole_grad, preferred_element_type=jnp.float32)
    summed_gate = lax.psum(local_gate.astype(jnp.bfloat16), "rep").astype(jnp.float32)
    summed_up = lax.psum(local_up.astype(jnp.bfloat16), "rep").astype(jnp.float32)
    summed_down = lax.psum(local_down.astype(jnp.bfloat16), "rep").astype(jnp.float32)
    grad_gate = summed_gate * factor
    grad_up = summed_up * factor
    grad_down = summed_down * (0.5 * factor)
    position = lax.axis_index("fs") * lax.axis_size("tp") + lax.axis_index("tp")
    own_unit = lax.dynamic_slice_in_dim(unit_rows, position * row_count, row_count, 0)
    own_inverse = lax.dynamic_slice_in_dim(inverse, position * row_count, row_count, 0)
    gain_local = jnp.sum(grad_normed * own_unit, axis=0)
    gain_partial = taken_together(gain_local, ("fs", "tp"))
    grad_gain = taken_together(gain_partial, "rep")
    scaled = grad_normed * norm_gain
    grad_in = (
        out_grad.astype(jnp.float32)
        + own_inverse * scaled
        - own_unit * own_inverse * jnp.mean(scaled * own_unit, axis=-1, keepdims=True)
    )
    return (grad_in.astype(jnp.bfloat16), grad_gain, grad_gate, grad_up, grad_down)


def solution(mesh):
    in_specs = (
        P(("rep", "fs", "tp"), None),
        P(),
        P(None, ("fs", "tp")),
        P(None, ("fs", "tp")),
        P(("fs", "tp"), None),
        P(("rep", "fs", "tp"), None),
    )
    out_specs = (
        P(("rep", "fs", "tp"), None),
        P(),
        P(None, ("fs", "tp")),
        P(None, ("fs", "tp")),
        P(("fs", "tp"), None),
    )
    return jax.shard_map(shards, mesh=mesh, in_specs=in_specs, out_specs=out_specs, check_vma=False)
```

profile of v0, /device:TPU:0, one launch (start us, length us, event | category | flops | bytes accessed | tf_op | source)
XLA Modules:
  0.0 341.8 jit_solution(17009870952825740865)
XLA Ops:
  8.0 0.7 all-gather.5.cloned.1.call-update
  8.7 53.2 %all-gather.3.cloned.1.call-done = bf16[2048,2048]{1,0:T(8,128)(2,1)} async-done(((bf16[256,2048]{1,0:T(8,128)(2,1)}), bf16[2048,2048]{1,0:T(8,128)(2,1)}) %all-gather.3.cloned.1.call-update) | async-done | bytes 8388624 | tf_op jit(solution)/shard_map/all_gather | solution.py:25
  61.9 5.2 %fusion = f32[2048]{0:T(1024)S(1)} fusion(bf16[2048,2048]{1,0:T(8,128)(2,1)} %all-gather.3.cloned.1.call-done), kind=kLoop, calls=%fused_computation.2 | loop fusion | flops 12580864 | bytes 8396800 | tf_op jit(solution)/shard_map/reduce_sum | solution.py:29
  67.7 6.3 %fusion.12 = f32[2048,384]{1,0:T(8,128)} fusion(bf16[2048,384]{1,0:T(8,128)(2,1)S(1)} %copy-done.3, f32[2048]{0:T(1024)S(1)} %copy-done.9, f32[2048]{0:T(1024)S(1)} %add_rsqrt_fusion, bf16[2048,2048]{1,0:T(8,128)(2,1)S(1)} %copy-done.1), kind=kOutput, calls=%fused_computation.30 | convolution fusion | flops 3238002688 | bytes 13123584 | tf_op jit(solution)/shard_map/dot_general | solution.py:33
  74.0 6.4 %fusion.11 = f32[2048,384]{1,0:T(8,128)} fusion(bf16[2048,384]{1,0:T(8,128)(2,1)S(1)} %copy-done, f32[2048]{0:T(1024)S(1)} %copy-done.9, f32[2048]{0:T(1024)S(1)} %add_rsqrt_fusion, bf16[2048,2048]{1,0:T(8,128)(2,1)S(1)} %copy-done.1), kind=kOutput, calls=%fused_computation.29 | convolution fusion | flops 3238002688 | bytes 13123584 | tf_op jit(solution)/shard_map/dot_general | solution.py:32
  80.4 33.1 %all-gather.5.cloned.1.call-done = bf16[2048,2048]{1,0:T(8,128)(2,1)} async-done(((bf16[256,2048]{1,0:T(8,128)(2,1)}), bf16[2048,2048]{1,0:T(8,128)(2,1)}) %all-gather.5.cloned.1.call-update) | async-done | bytes 8388624 | tf_op jit(solution)/shard_map/all_gather | solution.py:26
  113.5 10.3 %convolution_convert_fusion = bf16[384,2048]{1,0:T(8,128)(2,1)} fusion(bf16[2048,2048]{1,0:T(8,128)(2,1)} %all-gather.5.cloned.1.call-done, f32[2048,384]{1,0:T(8,128)} %fusion.12, f32[2048,384]{1,0:T(8,128)} %fusion.11), kind=kOutput, calls=%fused_computation.14 | convolution fusion | flops 3226730496 | bytes 16252928 | tf_op jit(solution)/shard_map/dot_general | solution.py:53
  123.8 7.5 %multiply_convert_fusion.2 = (bf16[2048,384]{1,0:T(8,128)(2,1)S(1)}, bf16[2048,384]{1,0:T(8,128)(2,1)S(1)}) fusion(f32[2048,384]{1,0:T(8,128)} %fusion.11, f32[2048,384]{1,0:T(8,128)S(1)} %copy-done.12, bf16[2048,2048]{1,0:T(8,128)(2,1)S(1)} %copy-done.10, bf16[384,2048]{1,0:T(8,128)(2,1)S(1)} %copy-done.11), kind=kOutput, calls=%fused_computation.9 | convolution fusion | flops 3232235520 | bytes 19398656 | tf_op jit(solution)/shard_map/dot_general | solution.py:37
  131.4 6.1 %convolution_convert_fusion.1 = bf16[2048,384]{1,0:T(8,128)(2,1)} fusion(bf16[2048,384]{1,0:T(8,128)(2,1)S(1)} %get-tuple-element.10, f32[2048]{0:T(1024)S(1)} %copy-done.9, f32[2048]{0:T(1024)S(1)} %add_rsqrt_fusion, bf16[2048,2048]{1,0:T(8,128)(2,1)S(1)} %bitcast.12), kind=kOutput, calls=%fused_computation.15 | convolution fusion | flops 3238789120 | bytes 11550720 | tf_op jit(solution)/shard_map/dot_general | solution.py:52
  137.5 6.1 %convolution_convert_fusion.2 = bf16[2048,384]{1,0:T(8,128)(2,1)} fusion(bf16[2048,384]{1,0:T(8,128)(2,1)S(1)} %get-tuple-element.11, f32[2048]{0:T(1024)S(1)} %copy-done.9, f32[2048]{0:T(1024)S(1)} %add_rsqrt_fusion, bf16[2048,2048]{1,0:T(8,128)(2,1)S(1)} %bitcast.12), kind=kOutput, calls=%fused_computation.16 | convolution fusion | flops 3238789120 | bytes 11550720 | tf_op jit(solution)/shard_map/dot_general | solution.py:51
  143.8 10.1 %fusion.13 = f32[2048,2048]{1,0:T(8,128)} fusion(bf16[2048,384]{1,0:T(8,128)(2,1)} %copy-done.8, bf16[2048,384]{1,0:T(8,128)(2,1)S(1)} %copy-done), kind=kOutput, calls=%fused_computation.31 | convolution fusion | flops 3221225472 | bytes 19922944 | tf_op jit(solution)/shard_map/dot_general | solution.py:42
  153.9 10.3 %add_convert_fusion = bf16[2048,2048]{1,0:T(8,128)(2,1)} fusion(f32[2048,2048]{1,0:T(8,128)} %fusion.13, bf16[2048,384]{1,0:T(8,128)(2,1)S(1)} %copy-done.7, bf16[2048,384]{1,0:T(8,128)(2,1)S(1)} %copy-done.3), kind=kOutput, calls=%fused_computation.3 | convolution fusion | flops 3229614080 | bytes 28311552 | tf_op jit(solution)/shard_map/dot_general | solution.py:44
  164.4 10.6 %convert_multiply_fusion = f32[2048,2048]{1,0:T(8,128)} fusion(bf16[2048,2048]{1,0:T(8,128)(2,1)} %all-gather.3.cloned.1.call-done, f32[2048]{0:T(1024)S(1)} %add_rsqrt_fusion), kind=kLoop, calls=%fused_computation | loop fusion | flops 8388608 | bytes 25174016 | tf_op jit(solution)/shard_map/mul | solution.py:30
  175.0 77.3 %all-reduce.3.cloned.1.call-done = (bf16[2048,384]{1,0:T(8,128)(2,1)}, bf16[2048,384]{1,0:T(8,128)(2,1)}, bf16[384,2048]{1,0:T(8,128)(2,1)}) async-done(((bf16[2048,384]{1,0:T(8,128)(2,1)}, bf16[2048,384]{1,0:T(8,128)(2,1)}, bf16[384,2048]{1,0:T(8,128)(2,1)}), (bf16[2048,384]{1,0:T(8,128)(2,1)}, bf16[2048,384]{1,0:T(8,128)(2,1)}, bf16[384,2048]{1,0:T(8,128)(2,1)})) %all-reduce.3.cloned.1.call-update) | async-done | bytes 4718608 | tf_op jit(solution)/shard_map/psum | solution.py:54
  252.3 3.6 %convert_multiply_fusion.2 = f32[384,2048]{1,0:T(8,128)} fusion(bf16[384,2048]{1,0:T(8,128)(2,1)} %get-tuple-element.9), kind=kLoop, calls=%fused_computation.5 | loop fusion | flops 1572864 | bytes 4718592 | tf_op jit(solution)/shard_map/mul | solution.py:59
  255.9 3.3 convert_multiply_fusion.3
  259.2 47.5 %reduce-scatter.2.cloned.1.call-done = bf16[256,2048]{1,0:T(8,128)(2,1)} async-done(((bf16[2048,2048]{1,0:T(8,128)(2,1)}), bf16[256,2048]{1,0:T(8,128)(2,1)}) %reduce-scatter.2.cloned.1.call-update) | async-done | bytes 1048592 | tf_op jit(solution)/shard_map/reduce_scatter | solution.py:43
  306.7 2.6 fusion.8
  309.9 3.4 all-to-all-start
  313.3 5.5 %all-to-all-done = f32[8,1,2048]{2,1,0:T(1,128)S(1)} async-done(((f32[8,1,2048]{2,1,0:T(1,128)}), f32[8,1,2048]{2,1,0:T(1,128)S(1)}, u32[]{:S(2)}, u32[]{:S(2)}) %all-to-all-start) | async-done | bytes 65568 | tf_op jit(solution)/shard_map/all_to_all | solution.py:11
  318.9 0.7 broadcast_in_dim.5
  319.6 6.9 %all-to-all-start.1 = ((f32[16,1,2048]{2,1,0:T(1,128)}), f32[16,1,2048]{2,1,0:T(1,128)S(1)}, u32[]{:S(2)}, u32[]{:S(2)}) async-start(f32[16,1,2048]{2,1,0:T(1,128)} %broadcast_in_dim.5), calls=%async_computation.2 | async-start | bytes 262144 | tf_op jit(solution)/shard_map/all_to_all | solution.py:11
  326.6 3.6 %fusion.6 = bf16[256,2048]{1,0:T(8,128)(2,1)} fusion(bf16[256,2048]{1,0:T(8,128)(2,1)} %reduce-scatter.2.cloned.1.call-done, bf16[256,2048]{1,0:T(8,128)(2,1)S(1)} %copy-done.2, f32[2048,2048]{1,0:T(8,128)} %convert_multiply_fusion, s32[]{:T(128)S(6)} %select_n.4, f32[256]{0:T(256)S(1)} %broadcast_multiply_fusion, f32[2048]{0:T(1024)S(1)} %copy-done.9, ...), kind=kLoop, calls=%fused_computation.23 | loop fusion | flops 4718592 | bytes 5253124 | tf_op jit(solution)/shard_map/convert_element_type | solution.py:72
  330.1 4.4 %all-to-all-done.1 = f32[16,1,2048]{2,1,0:T(1,128)S(1)} async-done(((f32[16,1,2048]{2,1,0:T(1,128)}), f32[16,1,2048]{2,1,0:T(1,128)S(1)}, u32[]{:S(2)}, u32[]{:S(2)}) %all-to-all-start.1) | async-done | bytes 131104 | tf_op jit(solution)/shard_map/all_to_all | solution.py:11
  (44 shorter events, 3.1 us)
Async XLA Ops:
  7.2 66.8 %copy-start = (bf16[2048,384]{1,0:T(8,128)(2,1)S(1)}, bf16[2048,384]{1,0:T(8,128)(2,1)}, u32[]{:S(2)}) copy-start(bf16[2048,384]{1,0:T(8,128)(2,1)} %param.8) | copy-start | bytes 4718596
  7.2 54.7 %all-gather.3.cloned.1.call-start = ((), (), s32[]{:S(2)}) async-start(), calls=%async_computation.3 | async-start | bytes 9437184 | tf_op jit(solution)/shard_map/all_gather | solution.py:25
  7.2 59.9 %copy-start.3 = (bf16[2048,384]{1,0:T(8,128)(2,1)S(1)}, bf16[2048,384]{1,0:T(8,128)(2,1)}, u32[]{:S(2)}) copy-start(bf16[2048,384]{1,0:T(8,128)(2,1)} %param.9) | copy-start | bytes 4718596
  7.9 105.6 %all-gather.5.cloned.1.call-start = ((), (), s32[]{:S(2)}) async-start(), calls=%async_computation.4 | async-start | bytes 9437184 | tf_op jit(solution)/shard_map/all_gather | solution.py:26
  8.7 58.5 %copy-start.9 = (f32[2048]{0:T(1024)S(1)}, f32[2048]{0:T(1024)}, u32[]{:S(2)}) copy-start(f32[2048]{0:T(1024)} %param.7) | copy-start | bytes 24580
  8.7 243.6 %all-reduce.3.cloned.1.call-start = ((), (), s32[]{:S(2)}) async-start(), calls=%async_computation.6 | async-start | bytes 9437184 | tf_op jit(solution)/shard_map/psum | solution.py:54
  61.9 5.8 %copy-start.1 = (bf16[2048,2048]{1,0:T(8,128)(2,1)S(1)}, bf16[2048,2048]{1,0:T(8,128)(2,1)}, u32[]{:S(2)}) copy-start(bf16[2048,2048]{1,0:T(8,128)(2,1)} %all-gather.3.cloned.1.call-done) | copy-start | bytes 25165828
  113.5 10.4 %copy-start.10 = (bf16[2048,2048]{1,0:T(8,128)(2,1)S(1)}, bf16[2048,2048]{1,0:T(8,128)(2,1)}, u32[]{:S(2)}) copy-start(bf16[2048,2048]{1,0:T(8,128)(2,1)} %all-gather.5.cloned.1.call-done) | copy-start | bytes 25165828
  113.5 10.4 %copy-start.11 = (bf16[384,2048]{1,0:T(8,128)(2,1)S(1)}, bf16[384,2048]{1,0:T(8,128)(2,1)}, u32[]{:S(2)}) copy-start(bf16[384,2048]{1,0:T(8,128)(2,1)} %param.10) | copy-start | bytes 4718596
  113.5 10.4 %copy-start.12 = (f32[2048,384]{1,0:T(8,128)S(1)}, f32[2048,384]{1,0:T(8,128)}, u32[]{:S(2)}) copy-start(f32[2048,384]{1,0:T(8,128)} %fusion.12) | copy-start | bytes 9437188
  113.5 17.9 %slice-start = ((s8[8388608]{0:T(1024)(128)(4,1)}), s8[4194304]{0:T(1024)(128)(4,1)S(1)}, s32[]{:S(2)}) async-start(s8[8388608]{0:T(1024)(128)(4,1)} %bitcast.11), calls=%async_computation.7 | async-start | bytes 8388608
  123.8 7.5 %slice-start.1 = ((s8[8388608]{0:T(1024)(128)(4,1)}), s8[4194304]{0:T(1024)(128)(4,1)S(1)}, s32[]{:S(2)}) async-start(s8[8388608]{0:T(1024)(128)(4,1)} %bitcast.11), calls=%async_computation.8 | async-start | bytes 8388608
  131.3 6.1 %copy-start.6 = (bf16[2048,384]{1,0:T(8,128)(2,1)}, bf16[2048,384]{1,0:T(8,128)(2,1)S(1)}, u32[]{:S(2)}) copy-start(bf16[2048,384]{1,0:T(8,128)(2,1)S(1)} %get-tuple-element.10) | copy-start | bytes 4718596
  131.3 6.1 %copy-start.8 = (bf16[2048,384]{1,0:T(8,128)(2,1)}, bf16[2048,384]{1,0:T(8,128)(2,1)S(1)}, u32[]{:S(2)}) copy-start(bf16[2048,384]{1,0:T(8,128)(2,1)S(1)} %get-tuple-element.11) | copy-start | bytes 4718596
  143.6 163.1 %reduce-scatter.2.cloned.1.call-start = ((), (), s32[]{:S(2)}) async-start(), calls=%async_computation.5 | async-start | bytes 9437184 | tf_op jit(solution)/shard_map/reduce_scatter | solution.py:43
  143.8 10.1 %copy-start.7 = (bf16[2048,384]{1,0:T(8,128)(2,1)S(1)}, bf16[2048,384]{1,0:T(8,128)(2,1)}, u32[]{:S(2)}) copy-start(bf16[2048,384]{1,0:T(8,128)(2,1)} %copy-done.6) | copy-start | bytes 4718596
  252.3 3.6 %copy-start.4 = (bf16[2048,384]{1,0:T(8,128)(2,1)S(1)}, bf16[2048,384]{1,0:T(8,128)(2,1)}, u32[]{:S(2)}) copy-start(bf16[2048,384]{1,0:T(8,128)(2,1)} %get-tuple-element.7) | copy-start | bytes 4718596
  252.3 3.6 %copy-start.5 = (bf16[2048,384]{1,0:T(8,128)(2,1)S(1)}, bf16[2048,384]{1,0:T(8,128)(2,1)}, u32[]{:S(2)}) copy-start(bf16[2048,384]{1,0:T(8,128)(2,1)} %get-tuple-element.8) | copy-start | bytes 4718596
  259.1 67.4 %copy-start.2 = (bf16[256,2048]{1,0:T(8,128)(2,1)S(1)}, bf16[256,2048]{1,0:T(8,128)(2,1)}, u32[]{:S(2)}) copy-start(bf16[256,2048]{1,0:T(8,128)(2,1)} %param.11) | copy-start | bytes 3145732
  309.9 8.9 %all-to-all-start = ((f32[8,1,2048]{2,1,0:T(1,128)}), f32[8,1,2048]{2,1,0:T(1,128)S(1)}, u32[]{:S(2)}, u32[]{:S(2)}) async-start(f32[8,1,2048]{2,1,0:T(1,128)} %broadcast_in_dim.4), calls=%async_computation.1 | async-start | bytes 131072 | tf_op jit(solution)/shard_map/all_to_all | solution.py:11
  319.6 14.9 %all-to-all-start.1 = ((f32[16,1,2048]{2,1,0:T(1,128)}), f32[16,1,2048]{2,1,0:T(1,128)S(1)}, u32[]{:S(2)}, u32[]{:S(2)}) async-start(f32[16,1,2048]{2,1,0:T(1,128)} %broadcast_in_dim.5), calls=%async_computation.2 | async-start | bytes 262144 | tf_op jit(solution)/shard_map/all_to_all | solution.py:11
Sparse Core Ops, SparseCore 0:
  9.7 52.1 all-gather.2
  63.6 49.8 all-gather.4
  143.7 108.5 all-reduce.2
  254.5 52.1 reduce-scatter.1
where the time goes:
time: 342 us
  waiting for transfers between devices  222 us (65%)
  matrix products  63.1 us (18%)
  other arithmetic  29.6 us (9%)
  between operations  13.9 us (4%)
  starting transfers between devices  10.7 us (3%)
    psum x1, waiting for transfers between devices, shards(): lax.psum(local_gate.astype(jnp.bfloat16), 'rep').astype(jnp.float32)  77.3 us
    all_gather x1, waiting for transfers between devices, shards(): lax.all_gather(tokens_in, ('fs', 'tp'), axis=0, tiled=True)  53.2 us
    reduce_scatter x1, waiting for transfers between devices, shards(): lax.psum_scatter((result + jnp.dot(grad_up_pre, up_weight.T, preferred_el...  47.5 us
    all_gather x1, waiting for transfers between devices, shards(): lax.all_gather(out_grad, ('fs', 'tp'), axis=0, tiled=True)  33.1 us
    mul x1, other arithmetic, shards(): unit_rows = floats * inverse  10.6 us
    dot_general x1, matrix products, shards(): jnp.dot(hidden.T, whole_grad, preferred_element_type=jnp.float32)  10.3 us
    dot_general x1, matrix products, shards(): jnp.dot(grad_up_pre, up_weight.T, preferred_element_type=jnp.float32)  10.3 us
    all_to_all x2, starting transfers between devices, sent_to_all(): lax.all_to_all(jnp.broadcast_to(value[None], (length, *value.shape)), axi...  10.3 us
  transfers between devices with their start and end apart: 6, of which 6 were waited for; matrix products, arithmetic and copies ran while one was open for 17% of the time, Pallas kernels for 0%

commit v1 on v0

v1 whole, which is shorter than its diff:
```python
import jax
import jax.numpy as jnp
from jax import lax
from jax.experimental import pallas as pl
from jax.experimental.pallas import tpu as pltpu
from jax.sharding import PartitionSpec as P

norm_eps = 1e-06
MESH = pl.DeviceIdType.MESH
F32 = jnp.float32
BF16 = jnp.bfloat16

D = 2048
FF = 384
ROWS = 256
PIECE = 64
HALF = 128
STEPS = 8
CH = 256
UNITS = (64, 96)
WIDTHS = (2 * FF, CH)


def over(n, step, body):
    def go(i, carry):
        body(pl.multiple_of(i * step, step))
        return carry

    lax.fori_loop(0, n // step, go, 0)


def dot(a, b, ca, cb):
    return lax.dot_general(a, b, (((ca,), (cb,)), ((), ())), preferred_element_type=F32)


def kernel(
    x_in, gain_in, gate_in, up_in, down_in, g_in,
    gin_out, gain_out, gu_out, dn_out,
    xg, wgu, wdn, gain, acc_gu, acc_dn, nrm, pre, gh, dgu, hid,
    kept, away, from_sib, far_l, far_r, near_l, near_r,
    wg, wd, s1g, s1d, t1g, t1d, vg, vd, s2g, s2d, t2g, t2d, og, od,
    g_tp, g_y, g_x, g_z,
    ld_sem, ag_send, ag_recv, sib_send, sib_recv, rs_send, rs_recv,
    ar_send, ar_recv, gn_send, gn_recv,
):
    rep, fs, tp = lax.axis_index("rep"), lax.axis_index("fs"), lax.axis_index("tp")
    z, x = rep // 4, rep % 4

    def y_at(k):
        return {"rep": rep, "fs": (fs + k) % 4, "tp": tp}

    def x_at(k):
        return {"rep": z * 4 + (x + k) % 4, "fs": fs, "tp": tp}

    def z_at(k):
        return {"rep": ((z + k) % 4) * 4 + x, "fs": fs, "tp": tp}

    sib = {"rep": rep, "fs": fs, "tp": 1 - tp}

    def remote(src, dst, send, recv, to):
        return pltpu.make_async_remote_copy(
            src_ref=src, dst_ref=dst, send_sem=send, recv_sem=recv, device_id=to, device_id_type=MESH
        )

    loads = []
    for s in range(2):
        loads.append(pltpu.make_async_copy(x_in.at[pl.ds(s * HALF, HALF)], xg.at[s, 0, pl.ds(0, HALF)], ld_sem.at[2 * s]))
        loads.append(pltpu.make_async_copy(g_in.at[pl.ds(s * HALF, HALF)], xg.at[s, 1, pl.ds(0, HALF)], ld_sem.at[2 * s + 1]))
    loads.append(pltpu.make_async_copy(gate_in, wgu.at[:, pl.ds(0, FF)], ld_sem.at[4]))
    loads.append(pltpu.make_async_copy(up_in, wgu.at[:, pl.ds(FF, FF)], ld_sem.at[5]))
    loads.append(pltpu.make_async_copy(down_in, wdn, ld_sem.at[6]))
    loads.append(pltpu.make_async_copy(gain_in, gain, ld_sem.at[7]))
    for c in loads:
        c.start()

    barrier = pltpu.get_barrier_semaphore()
    partners = [sib] + [at(k) for at in (y_at, x_at, z_at) for k in (1, 3, 2)]
    for p in partners:
        pl.semaphore_signal(barrier, inc=1, device_id=p, device_id_type=MESH)
    pl.semaphore_wait(barrier, len(partners))

    def to_sib(s):
        return remote(
            xg.at[s, :, pl.ds(0, HALF)], xg.at[s, :, pl.ds(HALF, HALF)], ag_send.at[s], ag_recv.at[s, 2], sib
        )

    def own_piece(p, j):
        src = xg.at[p // 2, :, pl.ds((p % 2) * PIECE, PIECE)]
        dst = xg.at[2 + p, :, pl.ds(j * PIECE, PIECE)]
        return remote(src, dst, ag_send.at[8 + 2 * p + j], ag_recv.at[2 + p, j], y_at(1 if j == 0 else 3))

    def onward(s, j):
        return remote(
            xg.at[s, :, pl.ds(j * PIECE, PIECE)],
            xg.at[s + 4 - 2 * j, :, pl.ds(j * PIECE, PIECE)],
            ag_send.at[14 + s],
            ag_recv.at[s + 4 - 2 * j, j],
            y_at(1 if j == 0 else 3),
        )

    def arrival(s, j):
        ref = xg.at[s, :, pl.ds(j * PIECE, PIECE)]
        return remote(ref, ref, ag_send.at[0], ag_recv.at[s, j], sib)

    for s in range(2):
        loads[2 * s].wait()
        loads[2 * s + 1].wait()
        for p in (2 * s, 2 * s + 1):
            own_piece(p, 0).start()
            own_piece(p, 1).start()
        to_sib(s).start()
    for c in loads[4:]:
        c.wait()

    def zero(r):
        acc_gu[pl.ds(r, 64), :] = jnp.zeros((64, 2 * FF), F32)
        acc_dn[pl.ds(pl.multiple_of(r // 64 * 96, 96), 96), :] = jnp.zeros((96, CH), F32)

    over(D, 64, zero)

    def sib_sum(s):
        return remote(away.at[s % 2], from_sib.at[s], sib_send.at[s % 2], sib_recv.at[s], sib)

    def chip_sum(s):
        sib_sum(s).wait_recv()

        def add(r):
            rows = pl.ds(r, 32)
            kept[s, rows, :] = (kept[s, rows, :].astype(F32) + from_sib[s, rows, :].astype(F32)).astype(BF16)

        over(HALF, 32, add)

    def early_right(q):
        return remote(kept.at[q, pl.ds(PIECE, PIECE)], near_l.at[q - 2], rs_send.at[q], rs_recv.at[0, q - 2], y_at(1))

    def early_left(q):
        return remote(kept.at[q, pl.ds(0, PIECE)], near_r.at[q - 2], rs_send.at[q], rs_recv.at[1, q - 2], y_at(3))

    def far_left(q):
        return remote(kept.at[q, pl.ds(0, PIECE)], far_r.at[q - 6], rs_send.at[q], rs_recv.at[2, q - 6], y_at(3))

    def far_right(q):
        return remote(kept.at[q, pl.ds(PIECE, PIECE)], far_l.at[q - 6], rs_send.at[q + 2], rs_recv.at[2, q - 4], y_at(1))

    def late_left(q):
        return remote(kept.at[q, pl.ds(0, PIECE)], near_r.at[q - 2], rs_send.at[q + 8], rs_recv.at[1, q - 2], y_at(3))

    def late_right(q):
        return remote(kept.at[q, pl.ds(PIECE, PIECE)], near_l.at[q - 2], rs_send.at[q + 8], rs_recv.at[0, q - 2], y_at(1))

    def step(s, carry):
        @pl.when(s >= 2)
        def _():
            arrival(s, 0).wait_recv()
            arrival(s, 1).wait_recv()
            to_sib(s).start()

        @pl.when((s == 2) | (s == 3))
        def _():
            onward(s, 0).start()

        @pl.when((s == 4) | (s == 5))
        def _():
            onward(s, 1).start()

        to_sib(s).wait_recv()

        def norm(r):
            rows = pl.ds(r, 16)
            floats = xg[s, 0, rows, :].astype(F32)
            inverse = lax.rsqrt(jnp.mean(floats * floats, axis=-1, keepdims=True) + norm_eps)
            nrm[rows, :] = (floats * inverse * gain[...]).astype(BF16)

        over(ROWS, 16, norm)
        pre[...] = dot(nrm[...], wgu[...], 1, 0)
        gh[...] = dot(xg[s, 1], wdn[...], 1, 1)

        def gates(r):
            rows = pl.ds(r, 32)
            gate_pre, up_pre = pre[rows, :FF], pre[rows, FF:]
            grad_hidden = 0.5 * gh[rows, :]
            sigma = jax.nn.sigmoid(gate_pre)
            active = gate_pre * sigma
            hid[rows, :] = (active * up_pre).astype(BF16)
            dgu[rows, :FF] = (grad_hidden * up_pre * sigma * (1.0 + gate_pre * (1.0 - sigma))).astype(BF16)
            dgu[rows, FF:] = (grad_hidden * active).astype(BF16)

        over(ROWS, 32, gates)

        @pl.when(s >= 2)
        def _():
            sib_sum(s).wait_send()

        def terms(c):
            cols = pl.ds(c, CH)
            term = dot(dgu[...], wgu[cols, :], 1, 1).astype(BF16)
            kept[s, :, cols] = term[:HALF]
            away[s % 2, :, cols] = term[HALF:]

        over(D, CH, terms)

        def weights(c):
            cols = pl.ds(c, CH)
            acc_gu[cols, :] += dot(nrm[:, cols], dgu[...], 0, 0)
            rows = pl.ds(pl.multiple_of(c // CH * FF, FF), FF)
            acc_dn[rows, :] += dot(hid[...], xg[s, 1, :, cols], 0, 0)

        over(D, CH, weights)
        sib_sum(s).start()

        @pl.when(s >= 1)
        def _():
            chip_sum(s - 1)

        @pl.when((s == 3) | (s == 4))
        def _():
            early_right(s - 1).start()

        @pl.when((s == 5) | (s == 6))
        def _():
            early_left(s - 1).start()

        return carry

    lax.fori_loop(0, STEPS, step, 0)

    packed = ((wg, s1g, t1g, vg, s2g, t2g, og, gu_out), (wd, s1d, t1d, vd, s2d, t2d, od, dn_out))
    halves = ((x, z, x_at, z_at), (z, x, z_at, x_at))
    streams = [(h, k) for k in range(2) for h in range(2)]

    class Ring:
        def __init__(self, h, k, src, base, size, mid, end, index, at, sem):
            self.src, self.size, self.mid, self.end = src, size, mid, end
            half = size // 2
            self.half = half
            f = h * 2 + k

            def rows(chunk, part):
                start = base + ((index + chunk) % 4) * size + part * half
                return pl.ds(pl.multiple_of(start, 16), half)

            self.rows = rows

            def copy(i, chunk, part, dst, to):
                return remote(src.at[rows(chunk, part)], dst, ar_send.at[f, sem + i], ar_recv.at[f, sem + i], at(to))

            self.first = [
                copy(0, 2, 0, mid.at[h, 1], 3),
                copy(1, 2, 1, mid.at[h, 0], 1),
                copy(2, 3, 1, end.at[h, 1, pl.ds(half, half)], 3),
                copy(3, 1, 0, end.at[h, 0, pl.ds(0, half)], 1),
            ]
            self.second = [
                copy(4, 3, 0, end.at[h, 1, pl.ds(0, half)], 3),
                copy(5, 1, 1, end.at[h, 0, pl.ds(half, half)], 1),
            ]
            self.h = h

        def issue(self):
            for c in self.first:
                c.start()

        def relay(self):
            h = self.h
            for i, (chunk, part, side) in enumerate(((3, 0, 1), (1, 1, 0))):
                self.first[i].wait_recv()
                rows = self.rows(chunk, part)
                self.src[rows, :] = (self.src[rows, :].astype(F32) + self.mid[h, side].astype(F32)).astype(BF16)
                self.second[i].start()

        def finish(self, store):
            h = self.h
            for c in self.first[2:] + self.second:
                c.wait_recv()
            for part in range(2):
                local = pl.ds(part * self.half, self.half)
                total = self.src[self.rows(0, part), :].astype(F32)
                total = total + self.end[h, 0, local, :].astype(F32) + self.end[h, 1, local, :].astype(F32)
                store(part, total.astype(BF16))

        def drain(self):
            for c in self.first + self.second:
                c.wait_send()

    rings1, rings2 = {}, {}
    for h, k in streams:
        w, s1, t1, v, s2, t2, o, out = packed[k]
        i1, i2, at1, at2 = halves[h]
        unit = UNITS[k]
        rings1[h, k] = Ring(h, k, w, h * 16 * unit, 4 * unit, s1, t1, i1, at1, 0)
        rings2[h, k] = Ring(h, k, v, h * 4 * unit, unit, s2, t2, i2, at2, 6)

    def cast_gu(r):
        wg[pl.ds(r, 64), :] = acc_gu[pl.ds(r, 64), :].astype(BF16)

    def cast_dn(r):
        wd[pl.ds(r, 96), :] = acc_dn[pl.ds(r, 96), :].astype(BF16)

    over(D, 64, cast_gu)
    for h in range(2):
        rings1[h, 0].issue()
    over(8 * FF, 96, cast_dn)
    far_left(6).start()
    far_right(6).start()
    for h in range(2):
        rings1[h, 1].issue()
    chip_sum(7)
    far_left(7).start()
    far_right(7).start()

    for h in range(2):
        rings1[h, 0].relay()

    def add_far(q, lo, far, wait):
        wait.wait_recv()

        def add(r):
            rows = pl.ds(lo + r, 32)
            kept[q, rows, :] = (kept[q, rows, :].astype(F32) + far[pl.ds(r, 32), :].astype(F32)).astype(BF16)

        over(PIECE, 32, add)

    for i in range(2):
        add_far(2 + i, 0, far_r.at[i], far_left(6 + i))
        late_left(2 + i).start()
        add_far(4 + i, PIECE, far_l.at[i], far_right(6 + i))
        late_right(4 + i).start()
    for h in range(2):
        rings1[h, 1].relay()

    def store_v(h, k):
        v, unit = packed[k][3], UNITS[k]

        def store(part, value):
            v[pl.ds(h * 4 * unit + part * 2 * unit, 2 * unit), :] = value

        return store

    def store_o(h, k):
        o, unit = packed[k][6], UNITS[k]

        def store(part, value):
            o[h, pl.ds(part * (unit // 2), unit // 2), :] = value

        return store

    for h, k in streams:
        rings1[h, k].finish(store_v(h, k))
        rings2[h, k].issue()
    for h, k in streams:
        rings2[h, k].relay()

    class Gather:
        def __init__(self, h, k, src, base, size, index, at, sem):
            out, f, half = packed[k][7], h * 2 + k, size // 2

            def where(chunk, part=None):
                start = base + ((index + chunk) % 4) * size
                if part is None:
                    return pl.ds(pl.multiple_of(start, 16), size)
                return pl.ds(pl.multiple_of(start + part * half, 16), half)

            mine = out.at[where(0)] if src is None else src
            self.own = []
            for i, to in enumerate((1, 3)):
                self.own.append(
                    remote(mine, out.at[where(0)], ar_send.at[f, sem + i], ar_recv.at[f, sem + i], at(to))
                )
            self.near = [
                remote(out.at[where(c)], out.at[where(c)], ar_send.at[f, sem + i], ar_recv.at[f, sem + i], at(1))
                for i, c in enumerate((3, 1))
            ]
            self.on = [
                remote(out.at[where(c, i)], out.at[where(c, i)], ar_send.at[f, sem + 2 + i], ar_recv.at[f, sem + 2 + i], at(to))
                for i, (c, to) in enumerate(((3, 1), (1, 3)))
            ]
            self.far = [
                remote(out.at[where(2, i)], out.at[where(2, i)], ar_send.at[f, sem + 2 + i], ar_recv.at[f, sem + 2 + i], at(1))
                for i in range(2)
            ]

        def issue(self):
            for c in self.own:
                c.start()

        def relay(self):
            for near, on in zip(self.near, self.on):
                near.wait_recv()
                on.start()

        def finish(self):
            for c in self.far:
                c.wait_recv()

        def drain(self):
            for c in self.own + self.on:
                c.wait_send()

    back2, back1, homes = {}, {}, {}
    for h, k in streams:
        i1, i2, at1, at2 = halves[h]
        unit, o, out = UNITS[k], packed[k][6], packed[k][7]
        base = (h * 4 + i1) * 4 * unit
        back2[h, k] = Gather(h, k, o.at[h], base, unit, i2, at2, 12)
        back1[h, k] = Gather(h, k, None, h * 16 * unit, 4 * unit, i1, at1, 16)
        homes[h, k] = pltpu.make_async_copy(
            o.at[h], out.at[pl.ds(pl.multiple_of(base + i2 * unit, 16), unit)], ar_send.at[h * 2 + k, 20]
        )

    for h, k in streams:
        rings2[h, k].finish(store_o(h, k))
        homes[h, k].start()
        back2[h, k].issue()

    late_left(2).wait_recv()
    late_left(3).wait_recv()
    early_left(4).wait_recv()
    early_left(5).wait_recv()
    early_right(2).wait_recv()
    early_right(3).wait_recv()
    late_right(4).wait_recv()
    late_right(5).wait_recv()
    g_tp[tp] = jnp.zeros((8, D), F32)

    def own_rows(i, carry):
        r = pl.multiple_of(i * 16, 16)
        s, p = i // 8, i // 4
        half, piece = pl.ds(pl.multiple_of((i % 8) * 16, 16), 16), pl.ds(pl.multiple_of((i % 4) * 16, 16), 16)
        grad = kept[s, half, :].astype(F32) + near_l[p, piece, :].astype(F32) + near_r[p, piece, :].astype(F32)
        floats = xg[s, 0, half, :].astype(F32)
        inverse = lax.rsqrt(jnp.mean(floats * floats, axis=-1, keepdims=True) + norm_eps)
        unit_rows = floats * inverse
        gained = grad * unit_rows
        g_tp[tp] += gained[:8] + gained[8:]
        scaled = grad * gain[...]
        mean = jnp.mean(scaled * unit_rows, axis=-1, keepdims=True)
        result = xg[s, 1, half, :].astype(F32) + inverse * scaled - unit_rows * inverse * mean
        gin_out[pl.ds(r, 16), :] = result.astype(BF16)
        return carry

    lax.fori_loop(0, ROWS // 16, own_rows, 0)

    gains = []

    def spread(buffer, index, targets, first):
        copies = [
            remote(buffer.at[index], buffer.at[index], gn_send.at[first + i], gn_recv.at[first + i], to)
            for i, to in enumerate(targets)
        ]
        gains.extend(copies)
        for c in copies:
            c.start()
        return copies

    g1 = spread(g_tp, tp, [sib], 0)
    for h, k in streams:
        back2[h, k].relay()
    g1[0].wait_recv()
    g_y[fs] = g_tp[0] + g_tp[1]
    g2 = spread(g_y, fs, [y_at(1), y_at(2), y_at(3)], 1)
    for h, k in streams:
        back2[h, k].finish()
        homes[h, k].wait()
        back1[h, k].issue()
    for c in g2:
        c.wait_recv()
    g_x[x] = (g_y[0] + g_y[1]) + (g_y[2] + g_y[3])
    g3 = spread(g_x, x, [x_at(1), x_at(2), x_at(3)], 4)
    for c in g3:
        c.wait_recv()
    g_z[z] = (g_x[0] + g_x[1]) + (g_x[2] + g_x[3])
    g4 = spread(g_z, z, [z_at(1), z_at(2), z_at(3)], 7)
    for c in g4:
        c.wait_recv()
    gain_out[...] = (g_z[0] + g_z[1]) + (g_z[2] + g_z[3])
    for h, k in streams:
        back1[h, k].relay()
    for h, k in streams:
        back1[h, k].finish()

    for s in range(STEPS):
        to_sib(s).wait_send()
    for p in range(4):
        own_piece(p, 0).wait_send()
        own_piece(p, 1).wait_send()
    for s in range(2, 6):
        onward(s, 0 if s < 4 else 1).wait_send()
    sib_sum(6).wait_send()
    sib_sum(7).wait_send()
    for q in (2, 3):
        early_right(q).wait_send()
        late_left(q).wait_send()
    for q in (4, 5):
        early_left(q).wait_send()
        late_right(q).wait_send()
    for q in (6, 7):
        far_left(q).wait_send()
        far_right(q).wait_send()
    for h, k in streams:
        rings1[h, k].drain()
        rings2[h, k].drain()
        back2[h, k].drain()
        back1[h, k].drain()
    for c in gains:
        c.wait_send()


def fused(tokens_in, norm_gain, gate_weight, up_weight, down_weight, out_grad):
    any_space = pl.BlockSpec(memory_space=pl.ANY)
    vmem = pl.BlockSpec(memory_space=pltpu.VMEM)
    (ug, ud), (cg, cd) = UNITS, WIDTHS
    dma = pltpu.SemaphoreType.DMA
    scratch = [
        pltpu.VMEM((STEPS, 2, ROWS, D), BF16),
        pltpu.VMEM((D, 2 * FF), BF16),
        pltpu.VMEM((FF, D), BF16),
        pltpu.VMEM((1, D), F32),
        pltpu.VMEM((D, 2 * FF), F32),
        pltpu.VMEM((8 * FF, CH), F32),
        pltpu.VMEM((ROWS, D), BF16),
        pltpu.VMEM((ROWS, 2 * FF), F32),
        pltpu.VMEM((ROWS, FF), F32),
        pltpu.VMEM((ROWS, 2 * FF), BF16),
        pltpu.VMEM((ROWS, FF), BF16),
        pltpu.VMEM((STEPS, HALF, D), BF16),
        pltpu.VMEM((2, HALF, D), BF16),
        pltpu.VMEM((STEPS, HALF, D), BF16),
        pltpu.VMEM((2, PIECE, D), BF16),
        pltpu.VMEM((2, PIECE, D), BF16),
        pltpu.VMEM((4, PIECE, D), BF16),
        pltpu.VMEM((4, PIECE, D), BF16),
        pltpu.VMEM((D, cg), BF16),
        pltpu.VMEM((8 * FF, cd), BF16),
        pltpu.VMEM((2, 2, 2 * ug, cg), BF16),
        pltpu.VMEM((2, 2, 2 * ud, cd), BF16),
        pltpu.VMEM((2, 2, 4 * ug, cg), BF16),
        pltpu.VMEM((2, 2, 4 * ud, cd), BF16),
        pltpu.VMEM((2 * 4 * ug, cg), BF16),
        pltpu.VMEM((2 * 4 * ud, cd), BF16),
        pltpu.VMEM((2, 2, ug // 2, cg), BF16),
        pltpu.VMEM((2, 2, ud // 2, cd), BF16),
        pltpu.VMEM((2, 2, ug, cg), BF16),
        pltpu.VMEM((2, 2, ud, cd), BF16),
        pltpu.VMEM((2, ug, cg), BF16),
        pltpu.VMEM((2, ud, cd), BF16),
        pltpu.VMEM((2, 8, D), F32),
        pltpu.VMEM((4, 8, D), F32),
        pltpu.VMEM((4, 8, D), F32),
        pltpu.VMEM((4, 8, D), F32),
        dma((8,)),
        dma((20,)),
        dma((STEPS, 3)),
        dma((2,)),
        dma((STEPS,)),
        dma((14,)),
        dma((3, 4)),
        dma((4, 21)),
        dma((4, 20)),
        dma((10,)),
        dma((10,)),
    ]
    return pl.pallas_call(
        kernel,
        name="fused",
        out_shape=(
            jax.ShapeDtypeStruct((ROWS, D), BF16),
            jax.ShapeDtypeStruct((8, D), F32),
            jax.ShapeDtypeStruct((D, 2 * FF), BF16),
            jax.ShapeDtypeStruct((8 * FF, CH), BF16),
        ),
        in_specs=[any_space] * 6,
        out_specs=(vmem, vmem, any_space, any_space),
        scratch_shapes=scratch,
        compiler_params=pltpu.CompilerParams(
            collective_id=0, has_side_effects=True, vmem_limit_bytes=66_000_000
        ),
    )(tokens_in, norm_gain.reshape(1, D), gate_weight, up_weight, down_weight, out_grad)


def shards(tokens_in, norm_gain, gate_weight, up_weight, down_weight, out_grad):
    row_count = tokens_in.shape[0]
    total_tokens = row_count * lax.axis_size("rep") * lax.axis_size("fs") * lax.axis_size("tp")
    factor = float(total_tokens) ** (-0.5)
    grad_in, gain8, gu, dn = fused(tokens_in, norm_gain, gate_weight, up_weight, down_weight, out_grad)
    grad_gain = jnp.sum(gain8, axis=0)
    grad_gate = gu[:, :FF].astype(F32) * factor
    grad_up = gu[:, FF:].astype(F32) * factor
    grad_down = jnp.swapaxes(dn.reshape(8, FF, CH), 0, 1).reshape(FF, D).astype(F32) * (0.5 * factor)
    return (grad_in, grad_gain, grad_gate, grad_up, grad_down)


def solution(mesh):
    in_specs = (
        P(("rep", "fs", "tp"), None),
        P(),
        P(None, ("fs", "tp")),
        P(None, ("fs", "tp")),
        P(("fs", "tp"), None),
        P(("rep", "fs", "tp"), None),
    )
    out_specs = (
        P(("rep", "fs", "tp"), None),
        P(),
        P(None, ("fs", "tp")),
        P(None, ("fs", "tp")),
        P(("fs", "tp"), None),
    )
    return jax.shard_map(shards, mesh=mesh, in_specs=in_specs, out_specs=out_specs, check_vma=False)
```

time: 342 us -> 179 us (0.52)
  waiting for transfers between devices: 222 us -> 0 us
  Pallas kernels: 0 us -> 169 us
  matrix products: 63.1 us -> 0 us
  other arithmetic: 29.6 us -> 6.99 us
  between operations: 13.9 us -> 0.66 us
  starting transfers between devices: 10.7 us -> 0 us
    pallas_call x0 -> x1, Pallas kernels: none -> 169 us  [fused(): pl.pallas_call(kernel, name='fused', out_shape=(jax.ShapeDtypeStruct((ROW...]
    all_gather x2 -> x0, waiting for transfers between devices: 86.3 us -> none  [the longest x1 53.2 us: shards(): lax.all_gather(tokens_in, ('fs', 'tp'), axis=0, tiled=True)]
    psum x1 -> x0, waiting for transfers between devices: 77.3 us -> none  [shards(): lax.psum(local_gate.astype(jnp.bfloat16), 'rep').astype(jnp.float32)]
    dot_general x8 -> x0, matrix products: 63.1 us -> none  [the longest x1 10.3 us: shards(): jnp.dot(hidden.T, whole_grad, preferred_element_type=jnp.float32)]
    reduce_scatter x1 -> x0, waiting for transfers between devices: 47.5 us -> none  [shards(): lax.psum_scatter((result + jnp.dot(grad_up_pre, up_weight.T, preferred_el...]
    mul x3 -> x2, other arithmetic: 17.5 us -> 5.54 us  [the longest x1 5.26 us: shards(): grad_up = gu[:, FF:].astype(F32) * factor]
    all_to_all x2 -> x0, starting transfers between devices: 10.3 us -> none  [sent_to_all(): lax.all_to_all(jnp.broadcast_to(value[None], (length, *value.shape)), axi...]
    all_to_all x2 -> x0, waiting for transfers between devices: 9.95 us -> none  [sent_to_all(): lax.all_to_all(jnp.broadcast_to(value[None], (length, *value.shape)), axi...]
  transfers between devices with their start and end apart: 6 -> 0, of which waited for: 6 -> 0; matrix products, arithmetic and copies ran while one was open for 17% -> 0% of each run, Pallas kernels for 0% -> 0%
where the time goes in v1:
time: 179 us
  Pallas kernels  169 us (94%)
  other arithmetic  6.99 us (4%)
  local copies, waits for them, and re-layouts  3.09 us (2%)
    pallas_call x1, Pallas kernels, fused(): pl.pallas_call(kernel, name='fused', out_shape=(jax.ShapeDtypeStruct((ROW...  169 us
    mul x1, other arithmetic, shards(): grad_up = gu[:, FF:].astype(F32) * factor  5.26 us

profile of v1, /device:TPU:0, one launch (start us, length us, event | category | flops | bytes accessed | tf_op | source)
XLA Modules:
  0.0 179.2 jit_solution(14799045631826374995)
XLA Ops:
  0.6 168.5 %fused.1 = (bf16[256,2048]{1,0:T(8,128)(2,1)}, f32[8,2048]{1,0:T(8,128)}, bf16[2048,768]{1,0:T(8,128)(2,1)}, bf16[3072,256]{1,0:T(8,128)(2,1)}) custom-call(bf16[256,2048]{1,0:T(8,128)(2,1)} %x_in.1, f32[1,2048]{1,0:T(1,128)} %bitcast.8, bf16[2048,384]{1,0:T(8,128)(2,1)} %gate_in.1, bf16[2048,384]{1,0:T(8,128)(2,1)} %up_in.1, bf16[384,2048]{1,0:T(8,128)(2,1)} %down_in.1, ...), custom_call_target="tpu_custom_call" | custom-call | tf_op jit(solution)/shard_map/fused/pallas_call | solution.py:562
  169.1 1.5 reduce_sum.9
  170.6 0.0 copy-start
  170.6 5.3 %convert_multiply_fusion.1 = (f32[2048,384]{1,0:T(8,128)}, f32[2048,384]{1,0:T(8,128)}) fusion(bf16[2048,768]{1,0:T(8,128)(2,1)} %get-tuple-element.11), kind=kLoop, calls=%fused_computation.1 | loop fusion | flops 3145728 | bytes 9437184 | tf_op jit(solution)/shard_map/mul | solution.py:587
  175.9 0.0 copy-done
  175.9 0.3 convert_multiply_fusion
  176.1 0.0 copy-start.1
  176.2 2.1 %copy.12 = f32[8,48,8,256]{3,2,0,1:T(8,128)} copy(f32[8,48,8,256]{3,2,1,0:T(8,128)S(1)} %bitcast.6) | data formatting | bytes 6291456 | tf_op jit(solution)/shard_map/mul | solution.py:588
  178.3 0.0 copy-done.1
  178.3 1.0 copy.14
Async XLA Ops:
  170.6 5.3 %copy-start = (bf16[3072,256]{1,0:T(8,128)(2,1)S(1)}, bf16[3072,256]{1,0:T(8,128)(2,1)}, u32[]{:S(2)}) copy-start(bf16[3072,256]{1,0:T(8,128)(2,1)} %get-tuple-element.12) | copy-start | bytes 4718596
  176.1 2.1 %copy-start.1 = (bf16[256,2048]{1,0:T(8,128)(2,1)S(1)}, bf16[256,2048]{1,0:T(8,128)(2,1)}, u32[]{:S(2)}) copy-start(bf16[256,2048]{1,0:T(8,128)(2,1)} %get-tuple-element.20) | copy-start | bytes 3145732

commit v2 on v1

v2 whole, which is shorter than its diff:
```python
import jax
import jax.numpy as jnp
from jax import lax
from jax.experimental import pallas as pl
from jax.experimental.pallas import tpu as pltpu
from jax.sharding import PartitionSpec as P

norm_eps = 1e-06
MESH = pl.DeviceIdType.MESH
scope = jax.named_scope
F32 = jnp.float32
BF16 = jnp.bfloat16

D = 2048
FF = 384
ROWS = 256
PIECE = 64
HALF = 128
STEPS = 8
CH = 256
WIDE = 512
UNITS = (64, 64, 96)
WIDTHS = (FF, FF, CH)


def over(n, step, body):
    def go(i, carry):
        body(pl.multiple_of(i * step, step))
        return carry

    lax.fori_loop(0, n // step, go, 0)


def dot(a, b, ca, cb):
    return lax.dot_general(a, b, (((ca,), (cb,)), ((), ())), preferred_element_type=F32)


def kernel(
    x_in, gain_in, gate_in, up_in, down_in, g_in,
    gin_out, gain_out, ga_out, up_out, dn_out,
    xg, wgu, wdn, wgu_t, gain, acc_gu, acc_dn, pre, gh, dgu, hid,
    kept, away, from_sib, far_l, far_r, near_l, near_r,
    wg, wd, s1g, s1d, t1g, t1d, vg, vd, s2g, s2d, t2g, t2d,
    g_acc, g_tp, g_y, g_rep,
    ld_sem, ag_send, ag_recv, ag7_send, ag7_recv, sib_send, sib_recv, rs_send, rs_recv,
    ar_send, ar_recv, gn_send, gn_recv,
):
    rep, fs, tp = lax.axis_index("rep"), lax.axis_index("fs"), lax.axis_index("tp")
    z, x = rep // 4, rep % 4

    def y_at(k):
        return {"rep": rep, "fs": (fs + k) % 4, "tp": tp}

    def x_at(k):
        return {"rep": z * 4 + (x + k) % 4, "fs": fs, "tp": tp}

    def z_at(k):
        return {"rep": ((z + k) % 4) * 4 + x, "fs": fs, "tp": tp}

    sib = {"rep": rep, "fs": fs, "tp": 1 - tp}

    def remote(src, dst, send, recv, to):
        return pltpu.make_async_remote_copy(
            src_ref=src, dst_ref=dst, send_sem=send, recv_sem=recv, device_id=to, device_id_type=MESH
        )

    loads = []
    for s in range(2):
        loads.append(pltpu.make_async_copy(x_in.at[pl.ds(s * HALF, HALF)], away.at[s], ld_sem.at[2 * s]))
        loads.append(pltpu.make_async_copy(g_in.at[pl.ds(s * HALF, HALF)], xg.at[s, 1, pl.ds(0, HALF)], ld_sem.at[2 * s + 1]))
    loads.append(pltpu.make_async_copy(gate_in, wgu.at[:, pl.ds(0, FF)], ld_sem.at[4]))
    loads.append(pltpu.make_async_copy(up_in, wgu.at[:, pl.ds(FF, FF)], ld_sem.at[5]))
    loads.append(pltpu.make_async_copy(down_in, wdn, ld_sem.at[6]))
    loads.append(pltpu.make_async_copy(gain_in, gain, ld_sem.at[7]))
    for c in loads:
        c.start()

    barrier = pltpu.get_barrier_semaphore()
    plane = [
        {"rep": ((z + k // 4) % 4) * 4 + (x + k % 4) % 4, "fs": fs, "tp": tp} for k in range(1, 16)
    ]
    partners = [sib] + [y_at(k) for k in (1, 3, 2)] + plane
    for p in partners:
        pl.semaphore_signal(barrier, inc=1, device_id=p, device_id_type=MESH)

    def to_sib(s):
        return remote(
            xg.at[s, :, pl.ds(0, HALF)], xg.at[s, :, pl.ds(HALF, HALF)], ag_send.at[s], ag_recv.at[s, 2], sib
        )

    def own_piece(p, j):
        src = xg.at[p // 2, :, pl.ds((p % 2) * PIECE, PIECE)]
        dst = xg.at[2 + p, :, pl.ds(j * PIECE, PIECE)]
        return remote(src, dst, ag_send.at[8 + 2 * p + j], ag_recv.at[2 + p, j], y_at(1 if j == 0 else 3))

    def onward(s, j):
        return remote(
            xg.at[s, :, pl.ds(j * PIECE, PIECE)],
            xg.at[s + 4 - 2 * j, :, pl.ds(j * PIECE, PIECE)],
            ag_send.at[14 + s],
            ag_recv.at[s + 4 - 2 * j, j],
            y_at(1 if j == 0 else 3),
        )

    def last_onward(j, q):
        rows = pl.ds(j * PIECE + q * 32, 32)
        return remote(
            xg.at[3 + 2 * j, :, rows], xg.at[7, :, rows], ag7_send.at[0, j, q], ag7_recv.at[0, j, q], y_at(1 if j == 0 else 3)
        )

    def last_to_sib(j, q):
        near, far = pl.ds(j * PIECE + q * 32, 32), pl.ds(HALF + j * PIECE + q * 32, 32)
        return remote(xg.at[7, :, near], xg.at[7, :, far], ag7_send.at[1, j, q], ag7_recv.at[1, j, q], sib)

    parts = [(j, q) for q in range(2) for j in range(2)]

    def arrival(s, j):
        ref = xg.at[s, :, pl.ds(j * PIECE, PIECE)]
        return remote(ref, ref, ag_send.at[0], ag_recv.at[s, j], sib)

    def norm(p):
        def rows16(i, carry):
            rows = pl.ds(pl.multiple_of((p % 2) * PIECE + i * 16, 16), 16)
            floats = away[p // 2, rows, :].astype(F32)
            inverse = lax.rsqrt(jnp.mean(floats * floats, axis=-1, keepdims=True) + norm_eps)
            xg[p // 2, 0, rows, :] = (floats * inverse * gain[...]).astype(BF16)
            return carry

        lax.fori_loop(0, PIECE // 16, rows16, 0, unroll=2)

    def leave(p):
        own_piece(p, 0).start()
        own_piece(p, 1).start()

    with scope("first"):
        loads[7].wait()
        loads[0].wait()
        norm(0)
        loads[1].wait()
    with scope("barrier"):
        pl.semaphore_wait(barrier, len(partners))
    leave(0)
    norm(1)
    loads[2].wait()
    norm(2)
    to_sib(0).start()
    leave(1)
    norm(3)
    loads[3].wait()
    leave(2)
    for c in loads[4:7]:
        c.wait()
    to_sib(1).start()
    leave(3)

    def turn(c):
        cols = pl.ds(c, CH)
        wgu_t[:, cols] = wgu[cols, :].T

    with scope("turn"):
        over(D, CH, turn)

    def zero(r):
        acc_gu[pl.ds(r, 64), :] = jnp.zeros((64, 2 * FF), F32)
        acc_dn[pl.ds(pl.multiple_of(r // 64 * 96, 96), 96), :] = jnp.zeros((96, CH), F32)

    with scope('zero'):
        over(D, 64, zero)

    def sib_sum(s):
        return remote(away.at[s % 2], from_sib.at[s], sib_send.at[s % 2], sib_recv.at[s], sib)

    def chip_sum(s):
        sib_sum(s).wait_recv()

        def add(r):
            rows = pl.ds(r, 32)
            kept[s, rows, :] = (kept[s, rows, :].astype(F32) + from_sib[s, rows, :].astype(F32)).astype(BF16)

        over(HALF, 32, add)

    def early_right(q):
        return remote(kept.at[q, pl.ds(PIECE, PIECE)], near_l.at[q - 2], rs_send.at[q], rs_recv.at[0, q - 2], y_at(1))

    def early_left(q):
        return remote(kept.at[q, pl.ds(0, PIECE)], near_r.at[q - 2], rs_send.at[q], rs_recv.at[1, q - 2], y_at(3))

    def far_left(q):
        return remote(kept.at[q, pl.ds(0, PIECE)], far_r.at[q - 6], rs_send.at[q], rs_recv.at[2, q - 6], y_at(3))

    def far_right(q):
        return remote(kept.at[q, pl.ds(PIECE, PIECE)], far_l.at[q - 6], rs_send.at[q + 2], rs_recv.at[2, q - 4], y_at(1))

    def late_left(q):
        return remote(kept.at[q, pl.ds(0, PIECE)], near_r.at[q - 2], rs_send.at[q + 8], rs_recv.at[1, q - 2], y_at(3))

    def late_right(q):
        return remote(kept.at[q, pl.ds(PIECE, PIECE)], near_l.at[q - 2], rs_send.at[q + 8], rs_recv.at[0, q - 2], y_at(1))

    packed = [(*(ref.at[k] for ref in (wg, s1g, t1g, vg, s2g, t2g)), out) for k, out in enumerate((ga_out, up_out))]
    packed.append((wd, s1d, t1d, vd, s2d, t2d, dn_out))
    halves = ((x, z, x_at, z_at), (z, x, z_at, x_at))
    streams = [(h, k) for k in range(3) for h in range(2)]

    class Ring:
        def __init__(self, h, k, src, base, size, mid, end, index, at, sem):
            self.src, self.size, self.mid, self.end = src, size, mid, end
            half = size // 2
            self.half = half
            f = h * 3 + k

            def rows(chunk, part):
                start = base + ((index + chunk) % 4) * size + part * half
                return pl.ds(pl.multiple_of(start, 16), half)

            self.rows = rows

            def copy(i, chunk, part, dst, to):
                return remote(src.at[rows(chunk, part)], dst, ar_send.at[f, sem + i], ar_recv.at[f, sem + i], at(to))

            self.first = [
                copy(0, 2, 0, mid.at[h, 1], 3),
                copy(1, 2, 1, mid.at[h, 0], 1),
                copy(2, 3, 1, end.at[h, 1, pl.ds(half, half)], 3),
                copy(3, 1, 0, end.at[h, 0, pl.ds(0, half)], 1),
            ]
            self.second = [
                copy(4, 3, 0, end.at[h, 1, pl.ds(0, half)], 3),
                copy(5, 1, 1, end.at[h, 0, pl.ds(half, half)], 1),
            ]
            self.h = h

        def issue(self):
            for c in self.first:
                c.start()

        def relay(self):
            h = self.h
            for i, (chunk, part, side) in enumerate(((3, 0, 1), (1, 1, 0))):
                self.first[i].wait_recv()
                rows = self.rows(chunk, part)
                self.src[rows, :] = (self.src[rows, :].astype(F32) + self.mid[h, side].astype(F32)).astype(BF16)
                self.second[i].start()

        def finish(self, store):
            h = self.h
            for c in self.first[2:] + self.second:
                c.wait_recv()
            for part in range(2):
                local = pl.ds(part * self.half, self.half)
                total = self.src[self.rows(0, part), :].astype(F32)
                total = total + self.end[h, 0, local, :].astype(F32) + self.end[h, 1, local, :].astype(F32)
                store(part, total.astype(BF16))

        def drain(self):
            for c in self.first + self.second:
                c.wait_send()

    rings1, rings2 = {}, {}
    for h, k in streams:
        w, s1, t1, v, s2, t2, out = packed[k]
        i1, i2, at1, at2 = halves[h]
        unit = UNITS[k]
        rings1[h, k] = Ring(h, k, w, h * 16 * unit, 4 * unit, s1, t1, i1, at1, 0)
        rings2[h, k] = Ring(h, k, v, h * 4 * unit, unit, s2, t2, i2, at2, 6)

    def step(s, carry):
        with scope("w_sib"):

            @pl.when(s < STEPS - 1)
            def _():
                to_sib(s).wait_recv()

            @pl.when(s == STEPS - 1)
            def _():
                for j, q in parts:
                    last_to_sib(j, q).wait_recv()

        with scope("pre"):
            pre[...] = dot(xg[s, 0], wgu[...], 1, 0)
        with scope("gh"):
            gh[...] = dot(xg[s, 1], wdn[...], 1, 1)

        def gates(r):
            rows = pl.ds(r, 32)
            gate_pre, up_pre = pre[rows, :FF], pre[rows, FF:]
            grad_hidden = 0.5 * gh[rows, :]
            sigma = jax.nn.sigmoid(gate_pre)
            active = gate_pre * sigma
            hid[rows, :] = (active * up_pre).astype(BF16)
            dgu[rows, :FF] = (grad_hidden * up_pre * sigma * (1.0 + gate_pre * (1.0 - sigma))).astype(BF16)
            dgu[rows, FF:] = (grad_hidden * active).astype(BF16)

        with scope("gates"):
            over(ROWS, 32, gates)

        def part_gu(c):
            cols = pl.ds(c, WIDE)
            return cols, acc_gu[cols, :] + dot(xg[s, 0, :, cols], dgu[...], 0, 0)

        def part_dn(c, store):
            value = dot(hid[...], xg[s, 1, :, pl.ds(c, WIDE)], 0, 0)
            for i in range(WIDE // CH):
                rows = pl.ds(pl.multiple_of((c // CH + i) * FF, FF), FF)
                store(rows, acc_dn[rows, :] + value[:, i * CH : (i + 1) * CH])

        @pl.when(s < STEPS - 1)
        def _():
            def keep_dn(rows, value):
                acc_dn[rows, :] = value

            def weights(c):
                cols, value = part_gu(c)
                acc_gu[cols, :] = value
                part_dn(c, keep_dn)

            with scope("weights"):
                over(D, WIDE, weights)

        @pl.when(s == STEPS - 1)
        def _():
            def last_gu(c):
                cols, value = part_gu(c)
                wg[0, cols, :] = value[:, :FF].astype(BF16)
                wg[1, cols, :] = value[:, FF:].astype(BF16)

            def last_dn(rows, value):
                wd[rows, :] = value.astype(BF16)

            for h in range(2):
                with scope("last_gu"):
                    over(D // 2, WIDE, lambda c: last_gu(c + h * (D // 2)))
                rings1[h, 0].issue()
            with scope("last_dn"):
                over(D, WIDE, lambda c: part_dn(c, last_dn))
            for h in range(2):
                with scope("relay10"):
                    rings1[h, 0].relay()
                rings1[h, 1].issue()

        @pl.when((s >= 1) & (s < STEPS - 2))
        def _():
            with scope("w_nbr"):
                arrival(s + 1, 0).wait_recv()
                arrival(s + 1, 1).wait_recv()
            to_sib(s + 1).start()

        @pl.when(s == STEPS - 2)
        def _():
            with scope("w_nbr"):
                for j, q in parts:
                    last_onward(j, q).wait_recv()
                    last_to_sib(j, q).start()

        @pl.when(s == 1)
        def _():
            onward(s + 1, 0).start()

        @pl.when(s == 3)
        def _():
            onward(s + 1, 1).start()

        @pl.when(s == 2)
        def _():
            for q in range(2):
                last_onward(0, q).start()

        @pl.when(s == 4)
        def _():
            for q in range(2):
                last_onward(1, q).start()

        @pl.when(s >= 2)
        def _():
            sib_sum(s).wait_send()

        def terms(c):
            cols = pl.ds(c, WIDE)
            term = dot(dgu[...], wgu_t[:, cols], 1, 0).astype(BF16)
            kept[s, :, cols] = term[:HALF]
            away[s % 2, :, cols] = term[HALF:]

        with scope("terms"):
            over(D, WIDE, terms)

        @pl.when(s >= 1)
        def _():
            with scope("chipsum"):
                chip_sum(s - 1)

        sib_sum(s).start()

        @pl.when((s == 3) | (s == 4))
        def _():
            early_right(s - 1).start()

        @pl.when((s == 5) | (s == 6))
        def _():
            early_left(s - 1).start()

        return carry

    lax.fori_loop(0, STEPS, step, 0)

    def add_far(q, lo, far, wait):
        wait.wait_recv()

        def add(r):
            rows = pl.ds(lo + r, 32)
            kept[q, rows, :] = (kept[q, rows, :].astype(F32) + far[pl.ds(r, 32), :].astype(F32)).astype(BF16)

        over(PIECE, 32, add)

    def store_v(h, k):
        v, unit = packed[k][3], UNITS[k]

        def store(part, value):
            v[pl.ds(h * 4 * unit + part * 2 * unit, 2 * unit), :] = value

        return store

    class Back:
        def __init__(self, h, k):
            i1, i2, at1, at2 = halves[h]
            out, f, unit = packed[k][6], h * 3 + k, UNITS[k]
            half = unit // 2

            def spot(ra, rb, part=None):
                a, b = (i1 + ra) % 4, (i2 + rb) % 4
                rows = half if part is not None else unit
                if k < 2:
                    start = ((h * 4 + a) * 4 + b) * unit + (part or 0) * half
                    return pl.ds(pl.multiple_of(start, 16), rows), slice(None)
                start = b * unit + (part or 0) * half
                return pl.ds(pl.multiple_of(start, 16), rows), pl.ds(pl.multiple_of((h * 4 + a) * CH, CH), CH)

            def copy(i, to, *where):
                view = out.at[spot(*where)]
                return remote(view, view, ar_send.at[f, 12 + i], ar_recv.at[f, 12 + i], to)

            self.out, self.spot = out, spot
            self.own2 = [copy(0, at2(1), 0, 0), copy(1, at2(3), 0, 0)]
            self.near2 = [copy(0, at2(1), 0, 3), copy(1, at2(3), 0, 1)]
            self.on2 = [copy(2, at2(1), 0, 3, 0), copy(3, at2(3), 0, 1, 1)]
            self.far2 = [copy(2, at2(1), 0, 2, 0), copy(3, at2(3), 0, 2, 1)]
            self.out1 = [[copy(4 + 2 * r, at1(1), 0, r), copy(5 + 2 * r, at1(3), 0, r)] for r in range(4)]
            self.left1 = [copy(4 + 2 * r, at1(1), 3, r) for r in range(4)]
            self.right1 = [copy(5 + 2 * r, at1(3), 1, r) for r in range(4)]
            self.on1 = {
                0: copy(12, at1(1), 3, 0),
                3: copy(13, at1(1), 3, 3),
                1: copy(14, at1(3), 1, 1),
                2: copy(15, at1(3), 1, 2),
            }
            self.far1 = [copy(i, at1(1), 2, r) for i, r in ((12, 0), (13, 3), (14, 1), (15, 2))]

        def store(self, part, value):
            self.out[self.spot(0, 0, part)] = value

        def send(self, r):
            for c in self.out1[r]:
                c.start()

        def begin(self):
            for c in self.own2:
                c.start()
            self.send(0)

        def middle(self):
            for near, on, r in zip(self.near2, self.on2, (3, 1)):
                near.wait_recv()
                on.start()
                self.send(r)

        def last(self):
            for c in self.far2:
                c.wait_recv()
            self.send(2)

        def pass_on(self, *which):
            for r in which:
                (self.left1 if r in (0, 3) else self.right1)[r].wait_recv()
                self.on1[r].start()

        def finish(self):
            for c in (self.left1[1], self.left1[2], self.right1[0], self.right1[3], *self.far1):
                c.wait_recv()

        def drain(self):
            for c in self.own2 + self.on2 + sum(self.out1, []) + list(self.on1.values()):
                c.wait_send()

    back = {(h, k): Back(h, k) for h, k in streams}

    def own_rows(i, carry):
        r = pl.multiple_of(i * 16, 16)
        s, p = i // 8, i // 4
        half, piece = pl.ds(pl.multiple_of((i % 8) * 16, 16), 16), pl.ds(pl.multiple_of((i % 4) * 16, 16), 16)
        grad = kept[s, half, :].astype(F32) + near_l[p, piece, :].astype(F32) + near_r[p, piece, :].astype(F32)
        floats = away[s, half, :].astype(F32)
        inverse = lax.rsqrt(jnp.mean(floats * floats, axis=-1, keepdims=True) + norm_eps)
        unit_rows = floats * inverse
        gained = grad * unit_rows
        g_acc[...] += gained[:8] + gained[8:]
        scaled = grad * gain[...]
        mean = jnp.mean(scaled * unit_rows, axis=-1, keepdims=True)
        result = xg[s, 1, half, :].astype(F32) + inverse * scaled - unit_rows * inverse * mean
        gin_out[pl.ds(r, 16), :] = result.astype(BF16)
        return carry


    gains = []

    def spread(buffer, index, targets, first):
        copies = [
            remote(buffer.at[index], buffer.at[index], gn_send.at[first + i], gn_recv.at[first + i], to)
            for i, to in enumerate(targets)
        ]
        gains.extend(copies)
        for c in copies:
            c.start()
        return copies

    def both(k, act):
        for h in range(2):
            act(h, k)

    def relay1(h, k):
        rings1[h, k].relay()

    def finish1(h, k):
        rings1[h, k].finish(store_v(h, k))
        rings2[h, k].issue()

    def relay2(h, k):
        rings2[h, k].relay()

    def finish2(h, k):
        rings2[h, k].finish(back[h, k].store)
        back[h, k].begin()

    def near2(h, k):
        back[h, k].middle()

    def far2(h, k):
        back[h, k].last()

    def pass0(h, k):
        back[h, k].pass_on(0)

    def pass1(h, k):
        back[h, k].pass_on(3, 1)

    def pass2(h, k):
        back[h, k].pass_on(2)

    def far1(h, k):
        back[h, k].finish()

    def run(name, k, act):
        with scope(f"{name}{k}"):
            both(k, act)

    far_left(6).start()
    far_right(6).start()
    with scope("chip7"):
        chip_sum(7)
    far_left(7).start()
    far_right(7).start()
    sib_sum(6).wait_send()
    sib_sum(7).wait_send()
    again = [pltpu.make_async_copy(x_in.at[pl.ds(s * HALF, HALF)], away.at[s], ld_sem.at[s]) for s in range(2)]
    for c in again:
        c.start()

    def far(i):
        with scope("far"):
            add_far(2 + i, 0, far_r.at[i], far_left(6 + i))
            late_left(2 + i).start()
            add_far(4 + i, PIECE, far_l.at[i], far_right(6 + i))
            late_right(4 + i).start()

    run("finish1", 0, finish1)
    for h in range(2):
        with scope("relay11"):
            rings1[h, 1].relay()
    run("relay2", 0, relay2)
    both(2, lambda h, k: rings1[h, k].issue())
    run("finish1", 1, finish1)
    far(0)
    run("finish2", 0, finish2)
    run("relay2", 1, relay2)
    run("near2", 0, near2)
    run("relay1", 2, relay1)
    run("pass0", 0, pass0)
    run("finish2", 1, finish2)
    run("far2", 0, far2)
    far(1)
    run("finish1", 2, finish1)
    run("near2", 1, near2)
    run("pass1", 0, pass1)
    run("pass0", 1, pass0)
    run("relay2", 2, relay2)
    run("far2", 1, far2)
    run("pass2", 0, pass2)
    run("finish2", 2, finish2)
    run("pass1", 1, pass1)
    with scope("w_rs"):
        for c in again:
            c.wait()
        for q in (2, 3):
            early_right(q).wait_recv()
            late_left(q).wait_recv()
        for q in (4, 5):
            early_left(q).wait_recv()
            late_right(q).wait_recv()
    with scope("own"):
        g_acc[...] = jnp.zeros((8, D), F32)
        lax.fori_loop(0, ROWS // 16, own_rows, 0, unroll=2)
        g_tp[tp] = jnp.sum(g_acc[...], axis=0, keepdims=True)
    g1 = spread(g_tp, tp, [sib], 0)
    run("near2", 2, near2)
    run("pass2", 1, pass2)
    with scope("g1"):
        g1[0].wait_recv()
        g_y[fs] = g_tp[0] + g_tp[1]
        g2 = spread(g_y, fs, [y_at(1), y_at(2), y_at(3)], 1)
    run("far2", 2, far2)
    run("pass0", 2, pass0)
    with scope("g2"):
        for c in g2:
            c.wait_recv()
        g_rep[rep] = (g_y[0] + g_y[1]) + (g_y[2] + g_y[3])
        g3 = spread(g_rep, rep, plane, 4)
    run("pass1", 2, pass1)
    run("pass2", 2, pass2)
    with scope("g3"):
        for c in g3:
            c.wait_recv()
        total = g_rep[0]
        for i in range(1, 16):
            total = total + g_rep[i]
        gain_out[...] = total
    run("far1", 0, far1)
    run("far1", 1, far1)
    run("far1", 2, far1)

    for s in range(STEPS - 1):
        to_sib(s).wait_send()
    for p in range(4):
        own_piece(p, 0).wait_send()
        own_piece(p, 1).wait_send()
    for s in (2, 4):
        onward(s, 0 if s < 4 else 1).wait_send()
    for j, q in parts:
        last_onward(j, q).wait_send()
        last_to_sib(j, q).wait_send()
    for q in (2, 3):
        early_right(q).wait_send()
        late_left(q).wait_send()
    for q in (4, 5):
        early_left(q).wait_send()
        late_right(q).wait_send()
    for q in (6, 7):
        far_left(q).wait_send()
        far_right(q).wait_send()
    for h, k in streams:
        rings1[h, k].drain()
        rings2[h, k].drain()
        back[h, k].drain()
    for c in gains:
        c.wait_send()


def fused(tokens_in, norm_gain, gate_weight, up_weight, down_weight, out_grad):
    any_space = pl.BlockSpec(memory_space=pl.ANY)
    vmem = pl.BlockSpec(memory_space=pltpu.VMEM)
    (ug, _, ud), (cg, _, cd) = UNITS, WIDTHS
    dma = pltpu.SemaphoreType.DMA
    scratch = [
        pltpu.VMEM((STEPS, 2, ROWS, D), BF16),
        pltpu.VMEM((D, 2 * FF), BF16),
        pltpu.VMEM((FF, D), BF16),
        pltpu.VMEM((2 * FF, D), BF16),
        pltpu.VMEM((1, D), F32),
        pltpu.VMEM((D, 2 * FF), F32),
        pltpu.VMEM((8 * FF, CH), F32),
        pltpu.VMEM((ROWS, 2 * FF), F32),
        pltpu.VMEM((ROWS, FF), F32),
        pltpu.VMEM((ROWS, 2 * FF), BF16),
        pltpu.VMEM((ROWS, FF), BF16),
        pltpu.VMEM((STEPS, HALF, D), BF16),
        pltpu.VMEM((2, HALF, D), BF16),
        pltpu.VMEM((STEPS, HALF, D), BF16),
        pltpu.VMEM((2, PIECE, D), BF16),
        pltpu.VMEM((2, PIECE, D), BF16),
        pltpu.VMEM((4, PIECE, D), BF16),
        pltpu.VMEM((4, PIECE, D), BF16),
        pltpu.VMEM((2, D, cg), BF16),
        pltpu.VMEM((8 * FF, cd), BF16),
        pltpu.VMEM((2, 2, 2, 2 * ug, cg), BF16),
        pltpu.VMEM((2, 2, 2 * ud, cd), BF16),
        pltpu.VMEM((2, 2, 2, 4 * ug, cg), BF16),
        pltpu.VMEM((2, 2, 4 * ud, cd), BF16),
        pltpu.VMEM((2, 2 * 4 * ug, cg), BF16),
        pltpu.VMEM((2 * 4 * ud, cd), BF16),
        pltpu.VMEM((2, 2, 2, ug // 2, cg), BF16),
        pltpu.VMEM((2, 2, ud // 2, cd), BF16),
        pltpu.VMEM((2, 2, 2, ug, cg), BF16),
        pltpu.VMEM((2, 2, ud, cd), BF16),
        pltpu.VMEM((8, D), F32),
        pltpu.VMEM((2, 1, D), F32),
        pltpu.VMEM((4, 1, D), F32),
        pltpu.VMEM((16, 1, D), F32),
        dma((8,)),
        dma((20,)),
        dma((STEPS, 3)),
        dma((2, 2, 2)),
        dma((2, 2, 2)),
        dma((2,)),
        dma((STEPS,)),
        dma((14,)),
        dma((3, 4)),
        dma((6, 28)),
        dma((6, 28)),
        dma((19,)),
        dma((19,)),
    ]
    return pl.pallas_call(
        kernel,
        name="fused",
        out_shape=(
            pltpu.VMEM((ROWS, D), BF16),
            pltpu.VMEM((1, D), F32),
            pltpu.VMEM((D, FF), BF16),
            pltpu.VMEM((D, FF), BF16),
            pltpu.VMEM((FF, D), BF16),
        ),
        in_specs=[any_space] * 6,
        out_specs=(vmem,) * 5,
        scratch_shapes=scratch,
        compiler_params=pltpu.CompilerParams(
            collective_id=0, has_side_effects=True, vmem_limit_bytes=60_800_000
        ),
    )(tokens_in, norm_gain.reshape(1, D), gate_weight, up_weight, down_weight, out_grad)


def shards(tokens_in, norm_gain, gate_weight, up_weight, down_weight, out_grad):
    row_count = tokens_in.shape[0]
    total_tokens = row_count * lax.axis_size("rep") * lax.axis_size("fs") * lax.axis_size("tp")
    factor = float(total_tokens) ** (-0.5)
    grad_in, gain_row, ga, up, dn = fused(tokens_in, norm_gain, gate_weight, up_weight, down_weight, out_grad)
    grad_gain = gain_row.reshape(D)
    grad_gate = ga.astype(F32) * factor
    grad_up = up.astype(F32) * factor
    grad_down = dn.astype(F32) * (0.5 * factor)
    return (grad_in, grad_gain, grad_gate, grad_up, grad_down)


def solution(mesh):
    in_specs = (
        P(("rep", "fs", "tp"), None),
        P(),
        P(None, ("fs", "tp")),
        P(None, ("fs", "tp")),
        P(("fs", "tp"), None),
        P(("rep", "fs", "tp"), None),
    )
    out_specs = (
        P(("rep", "fs", "tp"), None),
        P(),
        P(None, ("fs", "tp")),
        P(None, ("fs", "tp")),
        P(("fs", "tp"), None),
    )
    return jax.shard_map(shards, mesh=mesh, in_specs=in_specs, out_specs=out_specs, check_vma=False)
```

time: 179 us -> 153 us (0.85)
  Pallas kernels: 169 us -> 145 us
    pallas_call x1, Pallas kernels: 169 us -> 145 us  [fused(): pl.pallas_call(kernel, name='fused', out_shape=(pltpu.VMEM((ROWS, D), BF1...]
    mul x1 -> x0, local copies, waits for them, and re-layouts: 2.11 us -> none  [shards(): jnp.swapaxes(dn.reshape(8, FF, CH), 0, 1).reshape(FF, D).astype(F32)]
where the time goes in v2:
time: 153 us
  Pallas kernels  145 us (95%)
  other arithmetic  5.32 us (3%)
  local copies, waits for them, and re-layouts  1.57 us (1%)
    pallas_call x1, Pallas kernels, fused(): pl.pallas_call(kernel, name='fused', out_shape=(pltpu.VMEM((ROWS, D), BF1...  145 us
    mul x1, other arithmetic, shards(): grad_up = up.astype(F32) * factor  3.26 us

profile of v2, /device:TPU:0, one launch (start us, length us, event | category | flops | bytes accessed | tf_op | source)
XLA Modules:
  0.0 152.6 jit_solution(78774512661538312)
XLA Ops:
  0.6 145.1 %fused.1 = (bf16[256,2048]{1,0:T(8,128)(2,1)S(1)}, f32[1,2048]{1,0:T(1,128)S(1)}, bf16[2048,384]{1,0:T(8,128)(2,1)S(1)}, bf16[2048,384]{1,0:T(8,128)(2,1)S(1)}, bf16[384,2048]{1,0:T(8,128)(2,1)S(1)}) custom-call(bf16[256,2048]{1,0:T(8,128)(2,1)} %x_in.1, f32[1,2048]{1,0:T(1,128)} %bitcast.3, bf16[2048,384]{1,0:T(8,128)(2,1)} %gate_in.1, ...), custom_call_target="tpu_custom_call" | custom-call | tf_op jit(solution)/shard_map/fused/pallas_call | solution.py:729
  145.7 3.3 %convert_multiply_fusion.1 = (f32[2048,384]{1,0:T(8,128)}, f32[2048,384]{1,0:T(8,128)}) fusion(bf16[2048,384]{1,0:T(8,128)(2,1)S(1)} %get-tuple-element.13, bf16[2048,384]{1,0:T(8,128)(2,1)S(1)} %get-tuple-element.12), kind=kLoop, calls=%fused_computation.1 | loop fusion | flops 3145728 | bytes 9437184 | tf_op jit(solution)/shard_map/mul | solution.py:755
  149.0 2.1 %convert_multiply_fusion = f32[384,2048]{1,0:T(8,128)} fusion(bf16[384,2048]{1,0:T(8,128)(2,1)S(1)} %get-tuple-element.14), kind=kLoop, calls=%fused_computation | loop fusion | flops 1572864 | bytes 4718592 | tf_op jit(solution)/shard_map/mul | solution.py:756
  151.0 1.0 copy.13
  152.0 0.6 copy.14

commit v3 on v2

--- a/solution.py
+++ b/solution.py
@@ -1,3 +1,5 @@
+import functools
+
 import jax
 import jax.numpy as jnp
 from jax import lax
@@ -72,8 +74,8 @@
     loads.append(pltpu.make_async_copy(up_in, wgu.at[:, pl.ds(FF, FF)], ld_sem.at[5]))
     loads.append(pltpu.make_async_copy(down_in, wdn, ld_sem.at[6]))
     loads.append(pltpu.make_async_copy(gain_in, gain, ld_sem.at[7]))
-    for c in loads:
-        c.start()
+    for i in (7, 0, 1, 2, 3):
+        loads[i].start()
 
     barrier = pltpu.get_barrier_semaphore()
     plane = [
@@ -135,8 +137,10 @@
     with scope("first"):
         loads[7].wait()
         loads[0].wait()
+        loads[1].wait()
+        for c in loads[4:7]:
+            c.start()
         norm(0)
-        loads[1].wait()
     with scope("barrier"):
         pl.semaphore_wait(barrier, len(partners))
     leave(0)
@@ -230,8 +234,12 @@
             ]
             self.h = h
 
-        def issue(self):
-            for c in self.first:
+        def mid_out(self):
+            for c in self.first[:2]:
+                c.start()
+
+        def end_out(self):
+            for c in self.first[2:]:
                 c.start()
 
         def relay(self):
@@ -330,13 +338,11 @@
             for h in range(2):
                 with scope("last_gu"):
                     over(D // 2, WIDE, lambda c: last_gu(c + h * (D // 2)))
-                rings1[h, 0].issue()
+                rings1[h, 0].mid_out()
+                rings1[h, 1].mid_out()
+                rings1[h, 0].end_out()
             with scope("last_dn"):
                 over(D, WIDE, lambda c: part_dn(c, last_dn))
-            for h in range(2):
-                with scope("relay10"):
-                    rings1[h, 0].relay()
-                rings1[h, 1].issue()
 
         @pl.when((s >= 1) & (s < STEPS - 2))
         def _():
@@ -530,7 +536,8 @@
 
     def finish1(h, k):
         rings1[h, k].finish(store_v(h, k))
-        rings2[h, k].issue()
+        rings2[h, k].mid_out()
+        rings2[h, k].end_out()
 
     def relay2(h, k):
         rings2[h, k].relay()
@@ -580,31 +587,27 @@
             add_far(4 + i, PIECE, far_l.at[i], far_right(6 + i))
             late_right(4 + i).start()
 
+    run("relay1", 0, relay1)
+    run("relay1", 1, relay1)
+    both(2, lambda h, k: rings1[h, k].mid_out())
+    far(0)
     run("finish1", 0, finish1)
-    for h in range(2):
-        with scope("relay11"):
-            rings1[h, 1].relay()
+    both(1, lambda h, k: rings1[h, k].end_out())
+    both(2, lambda h, k: rings1[h, k].end_out())
     run("relay2", 0, relay2)
-    both(2, lambda h, k: rings1[h, k].issue())
+    run("relay1", 2, relay1)
     run("finish1", 1, finish1)
-    far(0)
     run("finish2", 0, finish2)
+    run("finish1", 2, finish1)
+    far(1)
     run("relay2", 1, relay2)
     run("near2", 0, near2)
-    run("relay1", 2, relay1)
-    run("pass0", 0, pass0)
+    run("relay2", 2, relay2)
     run("finish2", 1, finish2)
     run("far2", 0, far2)
-    far(1)
-    run("finish1", 2, finish1)
+    run("pass1", 0, pass1)
+    run("finish2", 2, finish2)
     run("near2", 1, near2)
-    run("pass1", 0, pass1)
-    run("pass0", 1, pass0)
-    run("relay2", 2, relay2)
-    run("far2", 1, far2)
-    run("pass2", 0, pass2)
-    run("finish2", 2, finish2)
-    run("pass1", 1, pass1)
     with scope("w_rs"):
         for c in again:
             c.wait()
@@ -620,20 +623,25 @@
         g_tp[tp] = jnp.sum(g_acc[...], axis=0, keepdims=True)
     g1 = spread(g_tp, tp, [sib], 0)
     run("near2", 2, near2)
-    run("pass2", 1, pass2)
     with scope("g1"):
         g1[0].wait_recv()
         g_y[fs] = g_tp[0] + g_tp[1]
         g2 = spread(g_y, fs, [y_at(1), y_at(2), y_at(3)], 1)
-    run("far2", 2, far2)
-    run("pass0", 2, pass0)
+    run("pass2", 0, pass2)
+    run("far2", 1, far2)
     with scope("g2"):
         for c in g2:
             c.wait_recv()
         g_rep[rep] = (g_y[0] + g_y[1]) + (g_y[2] + g_y[3])
         g3 = spread(g_rep, rep, plane, 4)
+    run("far2", 2, far2)
+    run("pass0", 0, pass0)
+    run("pass0", 1, pass0)
+    run("pass1", 1, pass1)
     run("pass1", 2, pass1)
+    run("pass2", 1, pass2)
     run("pass2", 2, pass2)
+    run("pass0", 2, pass0)
     with scope("g3"):
         for c in g3:
             c.wait_recv()
@@ -745,15 +753,53 @@
     )(tokens_in, norm_gain.reshape(1, D), gate_weight, up_weight, down_weight, out_grad)
 
 
+def scaled(factor, ga, up, dn, gin, gain, ga_out, up_out, dn_out, gin_out, gain_out, fa, fu, fd, sems):
+    copies = [
+        pltpu.make_async_copy(gin, gin_out, sems.at[0]),
+        pltpu.make_async_copy(gain, gain_out, sems.at[1]),
+    ]
+    for c in copies:
+        c.start()
+
+    def piece(i, src, mid, out, start, size, step, scale):
+        def convert(r):
+            rows = pl.ds(start + r, step)
+            mid[rows, :] = src[rows, :].astype(F32) * scale
+
+        over(size, step, convert)
+        rows = pl.ds(start, size)
+        copies.append(pltpu.make_async_copy(mid.at[rows], out.at[rows], sems.at[i]))
+        copies[-1].start()
+
+    for n in range(4):
+        piece(2 + n, ga, fa, ga_out, n * 512, 512, 64, factor)
+        piece(6 + n, up, fu, up_out, n * 512, 512, 64, factor)
+    for n in range(4):
+        piece(10 + n, dn, fd, dn_out, n * 96, 96, 16, 0.5 * factor)
+    for c in copies:
+        c.wait()
+
+
 def shards(tokens_in, norm_gain, gate_weight, up_weight, down_weight, out_grad):
     row_count = tokens_in.shape[0]
     total_tokens = row_count * lax.axis_size("rep") * lax.axis_size("fs") * lax.axis_size("tp")
     factor = float(total_tokens) ** (-0.5)
     grad_in, gain_row, ga, up, dn = fused(tokens_in, norm_gain, gate_weight, up_weight, down_weight, out_grad)
+    shapes = ((D, FF), (D, FF), (FF, D))
+    grad_gate, grad_up, grad_down, grad_in, gain_row = pl.pallas_call(
+        functools.partial(scaled, factor),
+        name="scaled",
+        out_shape=(
+            *(jax.ShapeDtypeStruct(shape, F32) for shape in shapes),
+            jax.ShapeDtypeStruct((ROWS, D), BF16),
+            jax.ShapeDtypeStruct((1, D), F32),
+        ),
+        in_specs=[pl.BlockSpec(memory_space=pltpu.VMEM)] * 5,
+        out_specs=(pl.BlockSpec(memory_space=pl.ANY),) * 5,
+        scratch_shapes=[*(pltpu.VMEM(shape, F32) for shape in shapes), pltpu.SemaphoreType.DMA((14,))],
+        compiler_params=pltpu.CompilerParams(vmem_limit_bytes=30_000_000),
+    )(*(pltpu.with_memory_space_constraint(v, pltpu.VMEM) for v in (ga, up, dn, grad_in, gain_row)))
     grad_gain = gain_row.reshape(D)
-    grad_gate = ga.astype(F32) * factor
-    grad_up = up.astype(F32) * factor
-    grad_down = dn.astype(F32) * (0.5 * factor)
     return (grad_in, grad_gain, grad_gate, grad_up, grad_down)
 
 

time: 153 us -> 145 us (0.948)
  other arithmetic: 5.32 us -> 0 us
  local copies, waits for them, and re-layouts: 1.57 us -> 0 us
    mul x2 -> x0, other arithmetic: 5.32 us -> none  [the longest x1 3.26 us: shards(): grad_up = up.astype(F32) * factor]
    pallas_call x1, Pallas kernels: 145 us -> 140 us  [fused(): pl.pallas_call(kernel, name='fused', out_shape=(pltpu.VMEM((ROWS, D), BF1...]
    pallas_call x0 -> x1, Pallas kernels: none -> 4.04 us  [shards(): pl.pallas_call(functools.partial(scaled, factor), name='scaled', out_shap...]
    unnamed x2 -> x0, local copies, waits for them, and re-layouts: 1.57 us -> none
where the time goes in v3:
time: 145 us
  Pallas kernels  144 us (99%)
    pallas_call x1, Pallas kernels, fused(): pl.pallas_call(kernel, name='fused', out_shape=(pltpu.VMEM((ROWS, D), BF1...  140 us
    pallas_call x1, Pallas kernels, shards(): pl.pallas_call(functools.partial(scaled, factor), name='scaled', out_shap...  4.04 us

profile of v3, /device:TPU:0, one launch (start us, length us, event | category | flops | bytes accessed | tf_op | source)
XLA Modules:
  0.0 144.8 jit_solution(17078876410346459118)
XLA Ops:
  0.6 140.1 %fused.1 = (bf16[256,2048]{1,0:T(8,128)(2,1)S(1)}, f32[1,2048]{1,0:T(1,128)S(1)}, bf16[2048,384]{1,0:T(8,128)(2,1)S(1)}, bf16[2048,384]{1,0:T(8,128)(2,1)S(1)}, bf16[384,2048]{1,0:T(8,128)(2,1)S(1)}) custom-call(bf16[256,2048]{1,0:T(8,128)(2,1)} %x_in.1, f32[1,2048]{1,0:T(1,128)} %bitcast.2, bf16[2048,384]{1,0:T(8,128)(2,1)} %gate_in.1, ...), custom_call_target="tpu_custom_call" | custom-call | tf_op jit(solution)/shard_map/fused/pallas_call | solution.py:737
  140.8 4.0 %scaled.1 = (f32[2048,384]{1,0:T(8,128)}, f32[2048,384]{1,0:T(8,128)}, f32[384,2048]{1,0:T(8,128)}, bf16[256,2048]{1,0:T(8,128)(2,1)}, f32[1,2048]{1,0:T(1,128)}) custom-call(bf16[2048,384]{1,0:T(8,128)(2,1)S(1)} %get-tuple-element.15.ga, bf16[2048,384]{1,0:T(8,128)(2,1)S(1)} %get-tuple-element.16.up, bf16[384,2048]{1,0:T(8,128)(2,1)S(1)} %get-tuple-element.17.dn, ...), custom_call_target="tpu_custom_call" | custom-call | tf_op jit(solution)/shard_map/scaled/pallas_call | solution.py:789

commit v4 on v3

--- a/solution.py
+++ b/solution.py
@@ -40,11 +40,11 @@
 def kernel(
     x_in, gain_in, gate_in, up_in, down_in, g_in,
     gin_out, gain_out, ga_out, up_out, dn_out,
-    xg, wgu, wdn, wgu_t, gain, acc_gu, acc_dn, pre, gh, dgu, hid,
+    xg, wg, wdn, wgu_t, gain, acc_gu, acc_dn, pre, gh, dgu, hid,
     kept, away, from_sib, far_l, far_r, near_l, near_r,
-    wg, wd, s1g, s1d, t1g, t1d, vg, vd, s2g, s2d, t2g, t2d,
+    wd, s1g, s1d, t1g, t1d, vg, vd, s2g, s2d, t2g, t2d,
     g_acc, g_tp, g_y, g_rep,
-    ld_sem, ag_send, ag_recv, ag7_send, ag7_recv, sib_send, sib_recv, rs_send, rs_recv,
+    ld_sem, ag_send, ag_recv, ag7_recv, sib_send, sib_recv, rs_send, rs_recv,
     ar_send, ar_recv, gn_send, gn_recv,
 ):
     rep, fs, tp = lax.axis_index("rep"), lax.axis_index("fs"), lax.axis_index("tp")
@@ -66,12 +66,15 @@
             src_ref=src, dst_ref=dst, send_sem=send, recv_sem=recv, device_id=to, device_id_type=MESH
         )
 
+    def taken(ref, sem):
+        pltpu.make_async_copy(ref, ref, sem).wait()
+
     loads = []
     for s in range(2):
         loads.append(pltpu.make_async_copy(x_in.at[pl.ds(s * HALF, HALF)], away.at[s], ld_sem.at[2 * s]))
         loads.append(pltpu.make_async_copy(g_in.at[pl.ds(s * HALF, HALF)], xg.at[s, 1, pl.ds(0, HALF)], ld_sem.at[2 * s + 1]))
-    loads.append(pltpu.make_async_copy(gate_in, wgu.at[:, pl.ds(0, FF)], ld_sem.at[4]))
-    loads.append(pltpu.make_async_copy(up_in, wgu.at[:, pl.ds(FF, FF)], ld_sem.at[5]))
+    loads.append(pltpu.make_async_copy(gate_in, wg.at[0], ld_sem.at[4]))
+    loads.append(pltpu.make_async_copy(up_in, wg.at[1], ld_sem.at[5]))
     loads.append(pltpu.make_async_copy(down_in, wdn, ld_sem.at[6]))
     loads.append(pltpu.make_async_copy(gain_in, gain, ld_sem.at[7]))
     for i in (7, 0, 1, 2, 3):
@@ -87,38 +90,43 @@
 
     def to_sib(s):
         return remote(
-            xg.at[s, :, pl.ds(0, HALF)], xg.at[s, :, pl.ds(HALF, HALF)], ag_send.at[s], ag_recv.at[s, 2], sib
+            xg.at[s, :, pl.ds(0, HALF)], xg.at[s, :, pl.ds(HALF, HALF)], ag_send, ag_recv.at[s, 1], sib
         )
 
     def own_piece(p, j):
         src = xg.at[p // 2, :, pl.ds((p % 2) * PIECE, PIECE)]
         dst = xg.at[2 + p, :, pl.ds(j * PIECE, PIECE)]
-        return remote(src, dst, ag_send.at[8 + 2 * p + j], ag_recv.at[2 + p, j], y_at(1 if j == 0 else 3))
+        return remote(src, dst, ag_send, ag_recv.at[2 + p, 0], y_at(1 if j == 0 else 3))
 
     def onward(s, j):
         return remote(
             xg.at[s, :, pl.ds(j * PIECE, PIECE)],
             xg.at[s + 4 - 2 * j, :, pl.ds(j * PIECE, PIECE)],
-            ag_send.at[14 + s],
-            ag_recv.at[s + 4 - 2 * j, j],
+            ag_send,
+            ag_recv.at[s + 4 - 2 * j, 0],
             y_at(1 if j == 0 else 3),
         )
 
     def last_onward(j, q):
-        rows = pl.ds(j * PIECE + q * 32, 32)
+        rows = pl.ds(j * PIECE, PIECE)
         return remote(
-            xg.at[3 + 2 * j, :, rows], xg.at[7, :, rows], ag7_send.at[0, j, q], ag7_recv.at[0, j, q], y_at(1 if j == 0 else 3)
+            xg.at[3 + 2 * j, q, rows], xg.at[7, q, rows], ag_send, ag7_recv.at[0, q], y_at(1 if j == 0 else 3)
         )
 
     def last_to_sib(j, q):
-        near, far = pl.ds(j * PIECE + q * 32, 32), pl.ds(HALF + j * PIECE + q * 32, 32)
-        return remote(xg.at[7, :, near], xg.at[7, :, far], ag7_send.at[1, j, q], ag7_recv.at[1, j, q], sib)
-
-    parts = [(j, q) for q in range(2) for j in range(2)]
-
-    def arrival(s, j):
-        ref = xg.at[s, :, pl.ds(j * PIECE, PIECE)]
-        return remote(ref, ref, ag_send.at[0], ag_recv.at[s, j], sib)
+        near, far = pl.ds(j * PIECE, PIECE), pl.ds(HALF + j * PIECE, PIECE)
+        return remote(xg.at[7, q, near], xg.at[7, q, far], ag_send, ag7_recv.at[1, q], sib)
+
+    def last_pass(q):
+        taken(xg.at[7, q, pl.ds(0, HALF)], ag7_recv.at[0, q])
+        for j in range(2):
+            last_to_sib(j, q).start()
+
+    def last_in(q):
+        taken(xg.at[7, q, pl.ds(HALF, HALF)], ag7_recv.at[1, q])
+
+    def arrival(s):
+        taken(xg.at[s, :, pl.ds(0, HALF)], ag_recv.at[s, 0])
 
     def norm(p):
         def rows16(i, carry):
@@ -159,7 +167,8 @@
 
     def turn(c):
         cols = pl.ds(c, CH)
-        wgu_t[:, cols] = wgu[cols, :].T
+        wgu_t[:FF, cols] = wg[0, cols, :].T
+        wgu_t[FF:, cols] = wg[1, cols, :].T
 
     with scope("turn"):
         over(D, CH, turn)
@@ -184,22 +193,22 @@
         over(HALF, 32, add)
 
     def early_right(q):
-        return remote(kept.at[q, pl.ds(PIECE, PIECE)], near_l.at[q - 2], rs_send.at[q], rs_recv.at[0, q - 2], y_at(1))
+        return remote(kept.at[q, pl.ds(PIECE, PIECE)], near_l.at[q - 2], rs_send, rs_recv.at[2], y_at(1))
 
     def early_left(q):
-        return remote(kept.at[q, pl.ds(0, PIECE)], near_r.at[q - 2], rs_send.at[q], rs_recv.at[1, q - 2], y_at(3))
+        return remote(kept.at[q, pl.ds(0, PIECE)], near_r.at[q - 2], rs_send, rs_recv.at[2], y_at(3))
 
     def far_left(q):
-        return remote(kept.at[q, pl.ds(0, PIECE)], far_r.at[q - 6], rs_send.at[q], rs_recv.at[2, q - 6], y_at(3))
+        return remote(kept.at[q, pl.ds(0, PIECE)], far_r.at[q - 6], rs_send, rs_recv.at[q - 6], y_at(3))
 
     def far_right(q):
-        return remote(kept.at[q, pl.ds(PIECE, PIECE)], far_l.at[q - 6], rs_send.at[q + 2], rs_recv.at[2, q - 4], y_at(1))
+        return remote(kept.at[q, pl.ds(PIECE, PIECE)], far_l.at[q - 6], rs_send, rs_recv.at[q - 6], y_at(1))
 
     def late_left(q):
-        return remote(kept.at[q, pl.ds(0, PIECE)], near_r.at[q - 2], rs_send.at[q + 8], rs_recv.at[1, q - 2], y_at(3))
+        return remote(kept.at[q, pl.ds(0, PIECE)], near_r.at[q - 2], rs_send, rs_recv.at[2], y_at(3))
 
     def late_right(q):
-        return remote(kept.at[q, pl.ds(PIECE, PIECE)], near_l.at[q - 2], rs_send.at[q + 8], rs_recv.at[0, q - 2], y_at(1))
+        return remote(kept.at[q, pl.ds(PIECE, PIECE)], near_l.at[q - 2], rs_send, rs_recv.at[2], y_at(1))
 
     packed = [(*(ref.at[k] for ref in (wg, s1g, t1g, vg, s2g, t2g)), out) for k, out in enumerate((ga_out, up_out))]
     packed.append((wd, s1d, t1d, vd, s2d, t2d, dn_out))
@@ -220,17 +229,20 @@
             self.rows = rows
 
             def copy(i, chunk, part, dst, to):
-                return remote(src.at[rows(chunk, part)], dst, ar_send.at[f, sem + i], ar_recv.at[f, sem + i], at(to))
+                return remote(src.at[rows(chunk, part)], dst, ar_send.at[f, sem], ar_recv.at[f, 2 * sem + i], at(to))
+
+            self.sems = ar_send.at[f, sem], ar_recv.at[f, 2 * sem], ar_recv.at[f, 2 * sem + 1]
+            self.bytes = lambda n: packed[k][0].at[pl.ds(0, n)]
 
             self.first = [
                 copy(0, 2, 0, mid.at[h, 1], 3),
-                copy(1, 2, 1, mid.at[h, 0], 1),
-                copy(2, 3, 1, end.at[h, 1, pl.ds(half, half)], 3),
-                copy(3, 1, 0, end.at[h, 0, pl.ds(0, half)], 1),
+                copy(0, 2, 1, mid.at[h, 0], 1),
+                copy(1, 3, 1, end.at[h, 1, pl.ds(half, half)], 3),
+                copy(1, 1, 0, end.at[h, 0, pl.ds(0, half)], 1),
             ]
             self.second = [
-                copy(4, 3, 0, end.at[h, 1, pl.ds(0, half)], 3),
-                copy(5, 1, 1, end.at[h, 0, pl.ds(half, half)], 1),
+                copy(1, 3, 0, end.at[h, 1, pl.ds(0, half)], 3),
+                copy(1, 1, 1, end.at[h, 0, pl.ds(half, half)], 1),
             ]
             self.h = h
 
@@ -244,16 +256,15 @@
 
         def relay(self):
             h = self.h
+            taken(self.bytes(self.size), self.sems[1])
             for i, (chunk, part, side) in enumerate(((3, 0, 1), (1, 1, 0))):
-                self.first[i].wait_recv()
                 rows = self.rows(chunk, part)
                 self.src[rows, :] = (self.src[rows, :].astype(F32) + self.mid[h, side].astype(F32)).astype(BF16)
                 self.second[i].start()
 
         def finish(self, store):
             h = self.h
-            for c in self.first[2:] + self.second:
-                c.wait_recv()
+            taken(self.bytes(2 * self.size), self.sems[2])
             for part in range(2):
                 local = pl.ds(part * self.half, self.half)
                 total = self.src[self.rows(0, part), :].astype(F32)
@@ -261,8 +272,7 @@
                 store(part, total.astype(BF16))
 
         def drain(self):
-            for c in self.first + self.second:
-                c.wait_send()
+            taken(self.bytes(3 * self.size), self.sems[0])
 
     rings1, rings2 = {}, {}
     for h, k in streams:
@@ -270,7 +280,7 @@
         i1, i2, at1, at2 = halves[h]
         unit = UNITS[k]
         rings1[h, k] = Ring(h, k, w, h * 16 * unit, 4 * unit, s1, t1, i1, at1, 0)
-        rings2[h, k] = Ring(h, k, v, h * 4 * unit, unit, s2, t2, i2, at2, 6)
+        rings2[h, k] = Ring(h, k, v, h * 4 * unit, unit, s2, t2, i2, at2, 1)
 
     def step(s, carry):
         with scope("w_sib"):
@@ -281,11 +291,18 @@
 
             @pl.when(s == STEPS - 1)
             def _():
-                for j, q in parts:
-                    last_to_sib(j, q).wait_recv()
+                last_in(0)
 
         with scope("pre"):
-            pre[...] = dot(xg[s, 0], wgu[...], 1, 0)
+            pre[:, :FF] = dot(xg[s, 0], wg[0], 1, 0)
+            pre[:, FF:] = dot(xg[s, 0], wg[1], 1, 0)
+
+        @pl.when(s == STEPS - 1)
+        def _():
+            with scope("w_last"):
+                last_pass(1)
+                last_in(1)
+
         with scope("gh"):
             gh[...] = dot(xg[s, 1], wdn[...], 1, 1)
 
@@ -302,8 +319,8 @@
         with scope("gates"):
             over(ROWS, 32, gates)
 
-        def part_gu(c):
-            cols = pl.ds(c, WIDE)
+        def part_gu(c, width):
+            cols = pl.ds(pl.multiple_of(c, width), width)
             return cols, acc_gu[cols, :] + dot(xg[s, 0, :, cols], dgu[...], 0, 0)
 
         def part_dn(c, store):
@@ -318,7 +335,7 @@
                 acc_dn[rows, :] = value
 
             def weights(c):
-                cols, value = part_gu(c)
+                cols, value = part_gu(c, WIDE)
                 acc_gu[cols, :] = value
                 part_dn(c, keep_dn)
 
@@ -328,35 +345,36 @@
         @pl.when(s == STEPS - 1)
         def _():
             def last_gu(c):
-                cols, value = part_gu(c)
+                cols, value = part_gu(c, CH)
                 wg[0, cols, :] = value[:, :FF].astype(BF16)
                 wg[1, cols, :] = value[:, FF:].astype(BF16)
 
             def last_dn(rows, value):
                 wd[rows, :] = value.astype(BF16)
 
-            for h in range(2):
+            for n in (2, 3, 1, 0):
                 with scope("last_gu"):
-                    over(D // 2, WIDE, lambda c: last_gu(c + h * (D // 2)))
-                rings1[h, 0].mid_out()
-                rings1[h, 1].mid_out()
-                rings1[h, 0].end_out()
+                    for h in range(2):
+                        last_gu((h * 4 + (halves[h][0] + n) % 4) * CH)
+                for h in range(2):
+                    if n == 2:
+                        rings1[h, 0].mid_out()
+                        rings1[h, 1].mid_out()
+                    if n == 1:
+                        rings1[h, 0].end_out()
             with scope("last_dn"):
                 over(D, WIDE, lambda c: part_dn(c, last_dn))
 
         @pl.when((s >= 1) & (s < STEPS - 2))
         def _():
             with scope("w_nbr"):
-                arrival(s + 1, 0).wait_recv()
-                arrival(s + 1, 1).wait_recv()
+                arrival(s + 1)
             to_sib(s + 1).start()
 
         @pl.when(s == STEPS - 2)
         def _():
             with scope("w_nbr"):
-                for j, q in parts:
-                    last_onward(j, q).wait_recv()
-                    last_to_sib(j, q).start()
+                last_pass(0)
 
         @pl.when(s == 1)
         def _():
@@ -408,9 +426,7 @@
 
     lax.fori_loop(0, STEPS, step, 0)
 
-    def add_far(q, lo, far, wait):
-        wait.wait_recv()
-
+    def add_far(q, lo, far):
         def add(r):
             rows = pl.ds(lo + r, 32)
             kept[q, rows, :] = (kept[q, rows, :].astype(F32) + far[pl.ds(r, 32), :].astype(F32)).astype(BF16)
@@ -442,23 +458,24 @@
 
             def copy(i, to, *where):
                 view = out.at[spot(*where)]
-                return remote(view, view, ar_send.at[f, 12 + i], ar_recv.at[f, 12 + i], to)
+                return remote(view, view, ar_send.at[f, 2], ar_recv.at[f, 4 + i], to)
+
+            self.taken = lambda units, sem: taken(packed[k][0].at[pl.ds(0, units * unit)], sem)
+            self.sems = ar_send.at[f, 2], [ar_recv.at[f, 4 + i] for i in range(6)]
 
             self.out, self.spot = out, spot
-            self.own2 = [copy(0, at2(1), 0, 0), copy(1, at2(3), 0, 0)]
-            self.near2 = [copy(0, at2(1), 0, 3), copy(1, at2(3), 0, 1)]
-            self.on2 = [copy(2, at2(1), 0, 3, 0), copy(3, at2(3), 0, 1, 1)]
-            self.far2 = [copy(2, at2(1), 0, 2, 0), copy(3, at2(3), 0, 2, 1)]
-            self.out1 = [[copy(4 + 2 * r, at1(1), 0, r), copy(5 + 2 * r, at1(3), 0, r)] for r in range(4)]
-            self.left1 = [copy(4 + 2 * r, at1(1), 3, r) for r in range(4)]
-            self.right1 = [copy(5 + 2 * r, at1(3), 1, r) for r in range(4)]
+            self.own2 = [copy(0, at2(1), 0, 0), copy(0, at2(3), 0, 0)]
+            self.on2 = [copy(1, at2(1), 0, 3, 0), copy(1, at2(3), 0, 1, 1)]
+            rightward, leftward = (2, 5, 5, 3), (5, 3, 4, 5)
+            self.out1 = [
+                [copy(rightward[r], at1(1), 0, r), copy(leftward[r], at1(3), 0, r)] for r in range(4)
+            ]
             self.on1 = {
-                0: copy(12, at1(1), 3, 0),
-                3: copy(13, at1(1), 3, 3),
-                1: copy(14, at1(3), 1, 1),
-                2: copy(15, at1(3), 1, 2),
+                0: copy(5, at1(1), 3, 0),
+                3: copy(5, at1(1), 3, 3),
+                1: copy(5, at1(3), 1, 1),
+                2: copy(5, at1(3), 1, 2),
             }
-            self.far1 = [copy(i, at1(1), 2, r) for i, r in ((12, 0), (13, 3), (14, 1), (15, 2))]
 
         def store(self, part, value):
             self.out[self.spot(0, 0, part)] = value
@@ -473,28 +490,25 @@
             self.send(0)
 
         def middle(self):
-            for near, on, r in zip(self.near2, self.on2, (3, 1)):
-                near.wait_recv()
+            self.taken(2, self.sems[1][0])
+            for on, r in zip(self.on2, (3, 1)):
                 on.start()
                 self.send(r)
 
         def last(self):
-            for c in self.far2:
-                c.wait_recv()
+            self.taken(1, self.sems[1][1])
             self.send(2)
 
         def pass_on(self, *which):
+            self.taken(len(which), self.sems[1][{0: 2, 3: 3, 2: 4}[which[0]]])
             for r in which:
-                (self.left1 if r in (0, 3) else self.right1)[r].wait_recv()
                 self.on1[r].start()
 
         def finish(self):
-            for c in (self.left1[1], self.left1[2], self.right1[0], self.right1[3], *self.far1):
-                c.wait_recv()
+            self.taken(8, self.sems[1][5])
 
         def drain(self):
-            for c in self.own2 + self.on2 + sum(self.out1, []) + list(self.on1.values()):
-                c.wait_send()
+            self.taken(15, self.sems[0])
 
     back = {(h, k): Back(h, k) for h, k in streams}
 
@@ -515,17 +529,13 @@
         return carry
 
 
-    gains = []
-
-    def spread(buffer, index, targets, first):
-        copies = [
-            remote(buffer.at[index], buffer.at[index], gn_send.at[first + i], gn_recv.at[first + i], to)
-            for i, to in enumerate(targets)
-        ]
-        gains.extend(copies)
-        for c in copies:
-            c.start()
-        return copies
+    def spread(buffer, index, targets, group):
+        for to in targets:
+            remote(buffer.at[index], buffer.at[index], gn_send.at[group], gn_recv.at[group], to).start()
+
+    def gathered(buffer, count, group):
+        for sems in (gn_recv, gn_send):
+            taken(buffer.at[pl.ds(0, count)], sems.at[group])
 
     def both(k, act):
         for h in range(2):
@@ -582,24 +592,40 @@
 
     def far(i):
         with scope("far"):
-            add_far(2 + i, 0, far_r.at[i], far_left(6 + i))
+            taken(kept.at[0], rs_recv.at[i])
+            add_far(2 + i, 0, far_r.at[i])
             late_left(2 + i).start()
-            add_far(4 + i, PIECE, far_l.at[i], far_right(6 + i))
+            add_far(4 + i, PIECE, far_l.at[i])
             late_right(4 + i).start()
+
+    def drain_gather():
+        taken(xg.at[pl.ds(0, 7)], ag_send)
+
+    def drain_tokens():
+        taken(kept.at[pl.ds(0, 6)], rs_send)
+
+    def drain_rings(rings, k):
+        both(k, lambda h, k: rings[h, k].drain())
+
+    def drain_out(k):
+        both(k, lambda h, k: back[h, k].drain())
 
     run("relay1", 0, relay1)
     run("relay1", 1, relay1)
     both(2, lambda h, k: rings1[h, k].mid_out())
-    far(0)
     run("finish1", 0, finish1)
     both(1, lambda h, k: rings1[h, k].end_out())
     both(2, lambda h, k: rings1[h, k].end_out())
+    far(0)
+    drain_gather()
     run("relay2", 0, relay2)
     run("relay1", 2, relay1)
     run("finish1", 1, finish1)
+    far(1)
+    drain_rings(rings1, 0)
+    drain_rings(rings1, 1)
     run("finish2", 0, finish2)
     run("finish1", 2, finish1)
-    far(1)
     run("relay2", 1, relay2)
     run("near2", 0, near2)
     run("relay2", 2, relay2)
@@ -607,34 +633,33 @@
     run("far2", 0, far2)
     run("pass1", 0, pass1)
     run("finish2", 2, finish2)
-    run("near2", 1, near2)
     with scope("w_rs"):
         for c in again:
             c.wait()
-        for q in (2, 3):
-            early_right(q).wait_recv()
-            late_left(q).wait_recv()
-        for q in (4, 5):
-            early_left(q).wait_recv()
-            late_right(q).wait_recv()
+        taken(kept.at[pl.ds(0, 4)], rs_recv.at[2])
     with scope("own"):
         g_acc[...] = jnp.zeros((8, D), F32)
         lax.fori_loop(0, ROWS // 16, own_rows, 0, unroll=2)
         g_tp[tp] = jnp.sum(g_acc[...], axis=0, keepdims=True)
-    g1 = spread(g_tp, tp, [sib], 0)
+    spread(g_tp, tp, [sib], 0)
+    run("near2", 1, near2)
+    drain_rings(rings1, 2)
+    drain_tokens()
     run("near2", 2, near2)
     with scope("g1"):
-        g1[0].wait_recv()
+        gathered(g_tp, 1, 0)
         g_y[fs] = g_tp[0] + g_tp[1]
-        g2 = spread(g_y, fs, [y_at(1), y_at(2), y_at(3)], 1)
+        spread(g_y, fs, [y_at(1), y_at(2), y_at(3)], 1)
     run("pass2", 0, pass2)
+    drain_rings(rings2, 0)
     run("far2", 1, far2)
+    drain_rings(rings2, 1)
+    drain_rings(rings2, 2)
+    run("far2", 2, far2)
     with scope("g2"):
-        for c in g2:
-            c.wait_recv()
+        gathered(g_y, 3, 1)
         g_rep[rep] = (g_y[0] + g_y[1]) + (g_y[2] + g_y[3])
-        g3 = spread(g_rep, rep, plane, 4)
-    run("far2", 2, far2)
+        spread(g_rep, rep, plane, 2)
     run("pass0", 0, pass0)
     run("pass0", 1, pass0)
     run("pass1", 1, pass1)
@@ -643,8 +668,7 @@
     run("pass2", 2, pass2)
     run("pass0", 2, pass0)
     with scope("g3"):
-        for c in g3:
-            c.wait_recv()
+        gathered(g_rep, 15, 2)
         total = g_rep[0]
         for i in range(1, 16):
             total = total + g_rep[i]
@@ -653,31 +677,8 @@
     run("far1", 1, far1)
     run("far1", 2, far1)
 
-    for s in range(STEPS - 1):
-        to_sib(s).wait_send()
-    for p in range(4):
-        own_piece(p, 0).wait_send()
-        own_piece(p, 1).wait_send()
-    for s in (2, 4):
-        onward(s, 0 if s < 4 else 1).wait_send()
-    for j, q in parts:
-        last_onward(j, q).wait_send()
-        last_to_sib(j, q).wait_send()
-    for q in (2, 3):
-        early_right(q).wait_send()
-        late_left(q).wait_send()
-    for q in (4, 5):
-        early_left(q).wait_send()
-        late_right(q).wait_send()
-    for q in (6, 7):
-        far_left(q).wait_send()
-        far_right(q).wait_send()
-    for h, k in streams:
-        rings1[h, k].drain()
-        rings2[h, k].drain()
-        back[h, k].drain()
-    for c in gains:
-        c.wait_send()
+    for k in range(3):
+        drain_out(k)
 
 
 def fused(tokens_in, norm_gain, gate_weight, up_weight, down_weight, out_grad):
@@ -687,7 +688,7 @@
     dma = pltpu.SemaphoreType.DMA
     scratch = [
         pltpu.VMEM((STEPS, 2, ROWS, D), BF16),
-        pltpu.VMEM((D, 2 * FF), BF16),
+        pltpu.VMEM((2, D, FF), BF16),
         pltpu.VMEM((FF, D), BF16),
         pltpu.VMEM((2 * FF, D), BF16),
         pltpu.VMEM((1, D), F32),
@@ -704,7 +705,6 @@
         pltpu.VMEM((2, PIECE, D), BF16),
         pltpu.VMEM((4, PIECE, D), BF16),
         pltpu.VMEM((4, PIECE, D), BF16),
-        pltpu.VMEM((2, D, cg), BF16),
         pltpu.VMEM((8 * FF, cd), BF16),
         pltpu.VMEM((2, 2, 2, 2 * ug, cg), BF16),
         pltpu.VMEM((2, 2, 2 * ud, cd), BF16),
@@ -721,18 +721,17 @@
         pltpu.VMEM((4, 1, D), F32),
         pltpu.VMEM((16, 1, D), F32),
         dma((8,)),
-        dma((20,)),
-        dma((STEPS, 3)),
-        dma((2, 2, 2)),
-        dma((2, 2, 2)),
+        dma,
+        dma((STEPS, 2)),
+        dma((2, 2)),
         dma((2,)),
         dma((STEPS,)),
-        dma((14,)),
-        dma((3, 4)),
-        dma((6, 28)),
-        dma((6, 28)),
-        dma((19,)),
-        dma((19,)),
+        dma,
+        dma((3,)),
+        dma((6, 3)),
+        dma((6, 10)),
+        dma((3,)),
+        dma((3,)),
     ]
     return pl.pallas_call(
         kernel,

time: 145 us -> 139 us (0.959)
  Pallas kernels: 144 us -> 138 us
    pallas_call x1, Pallas kernels: 140 us -> 134 us  [fused(): pl.pallas_call(kernel, name='fused', out_shape=(pltpu.VMEM((ROWS, D), BF1...]
where the time goes in v4:
time: 139 us
  Pallas kernels  138 us (99%)
    pallas_call x1, Pallas kernels, fused(): pl.pallas_call(kernel, name='fused', out_shape=(pltpu.VMEM((ROWS, D), BF1...  134 us
    pallas_call x1, Pallas kernels, shards(): pl.pallas_call(functools.partial(scaled, factor), name='scaled', out_shap...  4.04 us

profile of v4, /device:TPU:0, one launch (start us, length us, event | category | flops | bytes accessed | tf_op | source)
XLA Modules:
  0.0 138.6 jit_solution(8696790479391407624)
XLA Ops:
  0.6 133.9 %fused.1 = (bf16[256,2048]{1,0:T(8,128)(2,1)S(1)}, f32[1,2048]{1,0:T(1,128)S(1)}, bf16[2048,384]{1,0:T(8,128)(2,1)S(1)}, bf16[2048,384]{1,0:T(8,128)(2,1)S(1)}, bf16[384,2048]{1,0:T(8,128)(2,1)S(1)}) custom-call(bf16[256,2048]{1,0:T(8,128)(2,1)} %x_in.1, f32[1,2048]{1,0:T(1,128)} %bitcast.2, bf16[2048,384]{1,0:T(8,128)(2,1)} %gate_in.1, ...), custom_call_target="tpu_custom_call" | custom-call | tf_op jit(solution)/shard_map/fused/pallas_call | solution.py:736
  134.5 4.0 %scaled.1 = (f32[2048,384]{1,0:T(8,128)}, f32[2048,384]{1,0:T(8,128)}, f32[384,2048]{1,0:T(8,128)}, bf16[256,2048]{1,0:T(8,128)(2,1)}, f32[1,2048]{1,0:T(1,128)}) custom-call(bf16[2048,384]{1,0:T(8,128)(2,1)S(1)} %get-tuple-element.15.ga, bf16[2048,384]{1,0:T(8,128)(2,1)S(1)} %get-tuple-element.16.up, bf16[384,2048]{1,0:T(8,128)(2,1)S(1)} %get-tuple-element.17.dn, ...), custom_call_target="tpu_custom_call" | custom-call | tf_op jit(solution)/shard_map/scaled/pallas_call | solution.py:788

commit v5 on v4

--- a/solution.py
+++ b/solution.py
@@ -107,23 +107,27 @@
             y_at(1 if j == 0 else 3),
         )
 
+    parts = ((0, 0, PIECE), (1, 0, PIECE // 2), (1, PIECE // 2, PIECE // 2))
+
     def last_onward(j, q):
-        rows = pl.ds(j * PIECE, PIECE)
+        plane, low, count = parts[q]
+        rows = pl.ds(j * PIECE + low, count)
         return remote(
-            xg.at[3 + 2 * j, q, rows], xg.at[7, q, rows], ag_send, ag7_recv.at[0, q], y_at(1 if j == 0 else 3)
+            xg.at[3 + 2 * j, plane, rows], xg.at[7, plane, rows], ag_send, ag7_recv.at[0, q], y_at(1 if j == 0 else 3)
         )
 
     def last_to_sib(j, q):
-        near, far = pl.ds(j * PIECE, PIECE), pl.ds(HALF + j * PIECE, PIECE)
-        return remote(xg.at[7, q, near], xg.at[7, q, far], ag_send, ag7_recv.at[1, q], sib)
+        plane, low, count = parts[q]
+        near, far = pl.ds(j * PIECE + low, count), pl.ds(HALF + j * PIECE + low, count)
+        return remote(xg.at[7, plane, near], xg.at[7, plane, far], ag_send, ag7_recv.at[1, q], sib)
 
     def last_pass(q):
-        taken(xg.at[7, q, pl.ds(0, HALF)], ag7_recv.at[0, q])
+        taken(xg.at[7, parts[q][0], pl.ds(0, 2 * parts[q][2])], ag7_recv.at[0, q])
         for j in range(2):
             last_to_sib(j, q).start()
 
     def last_in(q):
-        taken(xg.at[7, q, pl.ds(HALF, HALF)], ag7_recv.at[1, q])
+        taken(xg.at[7, parts[q][0], pl.ds(HALF, 2 * parts[q][2])], ag7_recv.at[1, q])
 
     def arrival(s):
         taken(xg.at[s, :, pl.ds(0, HALF)], ag_recv.at[s, 0])
@@ -297,15 +301,6 @@
             pre[:, :FF] = dot(xg[s, 0], wg[0], 1, 0)
             pre[:, FF:] = dot(xg[s, 0], wg[1], 1, 0)
 
-        @pl.when(s == STEPS - 1)
-        def _():
-            with scope("w_last"):
-                last_pass(1)
-                last_in(1)
-
-        with scope("gh"):
-            gh[...] = dot(xg[s, 1], wdn[...], 1, 1)
-
         def gates(r):
             rows = pl.ds(r, 32)
             gate_pre, up_pre = pre[rows, :FF], pre[rows, FF:]
@@ -316,8 +311,28 @@
             dgu[rows, :FF] = (grad_hidden * up_pre * sigma * (1.0 + gate_pre * (1.0 - sigma))).astype(BF16)
             dgu[rows, FF:] = (grad_hidden * active).astype(BF16)
 
-        with scope("gates"):
-            over(ROWS, 32, gates)
+        def hidden_grads(low):
+            rows = pl.ds(low, HALF)
+            gh[rows, :] = dot(xg[s, 1, rows, :], wdn[...], 1, 1)
+            over(HALF, 32, lambda r: gates(low + r))
+
+        @pl.when(s == STEPS - 1)
+        def _():
+            with scope("w_last"):
+                last_pass(1)
+                last_pass(2)
+
+        with scope("gh"):
+            hidden_grads(0)
+
+        @pl.when(s == STEPS - 1)
+        def _():
+            with scope("w_last"):
+                last_in(1)
+                last_in(2)
+
+        with scope("gh"):
+            hidden_grads(HALF)
 
         def part_gu(c, width):
             cols = pl.ds(pl.multiple_of(c, width), width)
@@ -359,9 +374,9 @@
                 for h in range(2):
                     if n == 2:
                         rings1[h, 0].mid_out()
-                        rings1[h, 1].mid_out()
                     if n == 1:
                         rings1[h, 0].end_out()
+                        rings1[h, 1].mid_out()
             with scope("last_dn"):
                 over(D, WIDE, lambda c: part_dn(c, last_dn))
 
@@ -386,12 +401,12 @@
 
         @pl.when(s == 2)
         def _():
-            for q in range(2):
+            for q in range(3):
                 last_onward(0, q).start()
 
         @pl.when(s == 4)
         def _():
-            for q in range(2):
+            for q in range(3):
                 last_onward(1, q).start()
 
         @pl.when(s >= 2)
@@ -580,15 +595,6 @@
 
     far_left(6).start()
     far_right(6).start()
-    with scope("chip7"):
-        chip_sum(7)
-    far_left(7).start()
-    far_right(7).start()
-    sib_sum(6).wait_send()
-    sib_sum(7).wait_send()
-    again = [pltpu.make_async_copy(x_in.at[pl.ds(s * HALF, HALF)], away.at[s], ld_sem.at[s]) for s in range(2)]
-    for c in again:
-        c.start()
 
     def far(i):
         with scope("far"):
@@ -611,21 +617,30 @@
         both(k, lambda h, k: back[h, k].drain())
 
     run("relay1", 0, relay1)
+    both(2, lambda h, k: rings1[h, k].mid_out())
+    with scope("chip7"):
+        chip_sum(7)
+    far_left(7).start()
+    far_right(7).start()
     run("relay1", 1, relay1)
-    both(2, lambda h, k: rings1[h, k].mid_out())
+    sib_sum(6).wait_send()
+    sib_sum(7).wait_send()
+    again = [pltpu.make_async_copy(x_in.at[pl.ds(s * HALF, HALF)], away.at[s], ld_sem.at[s]) for s in range(2)]
+    for c in again:
+        c.start()
     run("finish1", 0, finish1)
     both(1, lambda h, k: rings1[h, k].end_out())
+    run("relay1", 2, relay1)
+    drain_gather()
+    run("relay2", 0, relay2)
     both(2, lambda h, k: rings1[h, k].end_out())
     far(0)
-    drain_gather()
-    run("relay2", 0, relay2)
-    run("relay1", 2, relay1)
     run("finish1", 1, finish1)
-    far(1)
     drain_rings(rings1, 0)
     drain_rings(rings1, 1)
     run("finish2", 0, finish2)
     run("finish1", 2, finish1)
+    far(1)
     run("relay2", 1, relay2)
     run("near2", 0, near2)
     run("relay2", 2, relay2)
@@ -651,6 +666,7 @@
         g_y[fs] = g_tp[0] + g_tp[1]
         spread(g_y, fs, [y_at(1), y_at(2), y_at(3)], 1)
     run("pass2", 0, pass2)
+    run("pass0", 1, pass0)
     drain_rings(rings2, 0)
     run("far2", 1, far2)
     drain_rings(rings2, 1)
@@ -660,13 +676,12 @@
         gathered(g_y, 3, 1)
         g_rep[rep] = (g_y[0] + g_y[1]) + (g_y[2] + g_y[3])
         spread(g_rep, rep, plane, 2)
-    run("pass0", 0, pass0)
-    run("pass0", 1, pass0)
     run("pass1", 1, pass1)
     run("pass1", 2, pass1)
     run("pass2", 1, pass2)
+    run("pass0", 2, pass0)
+    run("pass0", 0, pass0)
     run("pass2", 2, pass2)
-    run("pass0", 2, pass0)
     with scope("g3"):
         gathered(g_rep, 15, 2)
         total = g_rep[0]
@@ -723,7 +738,7 @@
         dma((8,)),
         dma,
         dma((STEPS, 2)),
-        dma((2, 2)),
+        dma((2, 3)),
         dma((2,)),
         dma((STEPS,)),
         dma,
@@ -770,11 +785,11 @@
         copies.append(pltpu.make_async_copy(mid.at[rows], out.at[rows], sems.at[i]))
         copies[-1].start()
 
-    for n in range(4):
-        piece(2 + n, ga, fa, ga_out, n * 512, 512, 64, factor)
-        piece(6 + n, up, fu, up_out, n * 512, 512, 64, factor)
-    for n in range(4):
-        piece(10 + n, dn, fd, dn_out, n * 96, 96, 16, 0.5 * factor)
+    for n in range(8):
+        piece(2 + n, ga, fa, ga_out, n * 256, 256, 64, factor)
+        piece(10 + n, up, fu, up_out, n * 256, 256, 64, factor)
+    for n in range(8):
+        piece(18 + n, dn, fd, dn_out, n * 48, 48, 16, 0.5 * factor)
     for c in copies:
         c.wait()
 
@@ -795,7 +810,7 @@
         ),
         in_specs=[pl.BlockSpec(memory_space=pltpu.VMEM)] * 5,
         out_specs=(pl.BlockSpec(memory_space=pl.ANY),) * 5,
-        scratch_shapes=[*(pltpu.VMEM(shape, F32) for shape in shapes), pltpu.SemaphoreType.DMA((14,))],
+        scratch_shapes=[*(pltpu.VMEM(shape, F32) for shape in shapes), pltpu.SemaphoreType.DMA((26,))],
         compiler_params=pltpu.CompilerParams(vmem_limit_bytes=30_000_000),
     )(*(pltpu.with_memory_space_constraint(v, pltpu.VMEM) for v in (ga, up, dn, grad_in, gain_row)))
     grad_gain = gain_row.reshape(D)

time: 139 us -> 139 us (level)
  no operation moved by 1% of the time
where the time goes in v5:
time: 139 us
  Pallas kernels  138 us (99%)
    pallas_call x1, Pallas kernels, fused(): pl.pallas_call(kernel, name='fused', out_shape=(pltpu.VMEM((ROWS, D), BF1...  134 us
    pallas_call x1, Pallas kernels, shards(): pl.pallas_call(functools.partial(scaled, factor), name='scaled', out_shap...  4.13 us

profile of v5, /device:TPU:0, one launch (start us, length us, event | category | flops | bytes accessed | tf_op | source)
XLA Modules:
  0.0 138.5 jit_solution(11787789334122061455)
XLA Ops:
  0.6 133.8 %fused.1 = (bf16[256,2048]{1,0:T(8,128)(2,1)S(1)}, f32[1,2048]{1,0:T(1,128)S(1)}, bf16[2048,384]{1,0:T(8,128)(2,1)S(1)}, bf16[2048,384]{1,0:T(8,128)(2,1)S(1)}, bf16[384,2048]{1,0:T(8,128)(2,1)S(1)}) custom-call(bf16[256,2048]{1,0:T(8,128)(2,1)} %x_in.1, f32[1,2048]{1,0:T(1,128)} %bitcast.2, bf16[2048,384]{1,0:T(8,128)(2,1)} %gate_in.1, ...), custom_call_target="tpu_custom_call" | custom-call | tf_op jit(solution)/shard_map/fused/pallas_call | solution.py:751
  134.4 4.1 %scaled.1 = (f32[2048,384]{1,0:T(8,128)}, f32[2048,384]{1,0:T(8,128)}, f32[384,2048]{1,0:T(8,128)}, bf16[256,2048]{1,0:T(8,128)(2,1)}, f32[1,2048]{1,0:T(1,128)}) custom-call(bf16[2048,384]{1,0:T(8,128)(2,1)S(1)} %get-tuple-element.15.ga, bf16[2048,384]{1,0:T(8,128)(2,1)S(1)} %get-tuple-element.16.up, bf16[384,2048]{1,0:T(8,128)(2,1)S(1)} %get-tuple-element.17.dn, ...), custom_call_target="tpu_custom_call" | custom-call | tf_op jit(solution)/shard_map/scaled/pallas_call | solution.py:803
